TPU v7x, 256 devices: a whole 4x4x8 slice. The times are simulated.
256 devices in a mesh: sp: 64 (over z, y, core), tp: 4 (over x).
Axes of the slice: x: 4, y: 4, z: 8, core: 2. Of those that a mesh axis runs over, the one named last changes fastest.
Arguments:
- stream_in: bfloat16 [16384, 4096], P(('sp', 'tp')), may hold values from -6 to 6
- q_first: bfloat16 [16384, 1024], P('sp', 'tp'), may hold values from -110 to 110
- q_second: bfloat16 [16384, 1024], P('sp', 'tp'), may hold values from -110 to 110
- k_first: bfloat16 [16384, 512], P('sp', 'tp'), may hold values from -7 to 7
- k_second: bfloat16 [16384, 512], P('sp', 'tp'), may hold values from -7 to 7
- values: bfloat16 [16384, 1024], P('sp', 'tp'), may hold values from -6 to 6
- head_lambda: float32 [8], P('tp'), may hold values from 0.3 to 0.8
- w_out: bfloat16 [2048, 4096], P('tp'), may hold values from -0.125 to 0.125
- norm_gain: float32 [4096], replicated, may hold values from 0.1 to 1.9
- routes: int32 [16384, 4], P(('sp', 'tp')), may hold values from 0 to 63, all different within a row; in each aligned block of 64 rows (0 to 63, 64 to 127, ...) at most 6 rows name the same one
- route_w: float32 [16384, 4], P(('sp', 'tp')), may hold values from 0.2 to 1
- w_gate: bfloat16 [64, 4096, 128], P('sp'), may hold values from -0.09375 to 0.09375
- w_up: bfloat16 [64, 4096, 128], P('sp'), may hold values from -0.09375 to 0.09375
- w_down: bfloat16 [64, 128, 4096], P('sp'), may hold values from -0.5 to 0.5
- s_gate: bfloat16 [4096, 512], P(None, 'tp'), may hold values from -0.09375 to 0.09375
- s_up: bfloat16 [4096, 512], P(None, 'tp'), may hold values from -0.09375 to 0.09375
- s_down: bfloat16 [512, 4096], P('tp'), may hold values from -0.25 to 0.25
Outputs:
- layer_out: bfloat16 [16384, 4096], P(('sp', 'tp'))
Inputs may be any that keep to these rules, and one draw needn't show every extreme that they name: `routes`: each row names 4 different experts. Within the rows of one device (aligned blocks of 64 rows) no expert is named more than 6 times, and in some blocks one expert is named exactly 6 times.
All inputs are finite; a program needn't handle non-finite values.
Results may differ from a plain program's by a relative error of at most 0.017.
Values may be sent and summed in bfloat16 or wider, within the bound.
A program may use at most 128 MiB of HBM per device.

v0:
```python
import math

import jax
import jax.numpy as jnp
from jax import lax
from jax.sharding import PartitionSpec as P

HEAD = 128


FLOOR = -1e30


def side_by_side(arrays, axis, dim, along):
    widths = [a.shape[along] for a in arrays]
    both = jnp.concatenate(arrays, axis=along)
    out = lax.all_gather(both, axis, axis=dim, tiled=True)
    return tuple(jnp.split(out, [sum(widths[:k]) for k in range(1, len(widths))], axis=along))


def cut_along(x, dim, count):
    shape = x.shape
    pieces = x.reshape(*shape[:dim], count, shape[dim] // count, *shape[dim + 1 :])
    return jnp.moveaxis(pieces, dim, 0)


def sum_at_owner(x, axis, dim):
    count = lax.axis_size(axis)
    pieces = lax.all_to_all(cut_along(x, dim, count), axis, 0, 0, tiled=True)
    return jnp.sum(pieces.astype(jnp.float32), axis=0)


def absorb(state, first_q, second_q, first_k, second_k, value_rows, query_pos, key_pos):
    allowed = key_pos[None, :] <= query_pos[:, None]
    scale = first_q.shape[-1] ** (-0.5)
    result = []
    pairs = ((first_q, first_k), (second_q, second_k))
    for index in range(2):
        query_rows, key_rows = pairs[index]
        peak, total, accum = (state[3 * index], state[3 * index + 1], state[3 * index + 2])
        scores = (
            jnp.einsum("qagd,kad->agqk", query_rows, key_rows, preferred_element_type=jnp.float32)
            * scale
        )
        scores = jnp.where(allowed, scores, FLOOR)
        raised = jnp.maximum(peak, scores.max(-1))
        weights = jnp.where(allowed, jnp.exp(scores - raised[..., None]), 0.0)
        fade = jnp.exp(peak - raised)
        total = total * fade + weights.sum(-1)
        accum = accum * fade[..., None] + jnp.einsum(
            "agqk,kad->agqd",
            weights.astype(jnp.bfloat16),
            value_rows,
            preferred_element_type=jnp.float32,
        )
        result += [raised, total, accum]
    return tuple(result)


def empty_state(kv_local, group, count, value_dim):
    peaks = jnp.full((kv_local, group, count), FLOOR, jnp.float32)
    sums = jnp.zeros((kv_local, group, count), jnp.float32)
    accums = jnp.zeros((kv_local, group, count, value_dim), jnp.float32)
    return (peaks, sums, accums, peaks, sums, accums)


def fold_rows(state, first_q, second_q, query_pos, last_row, pieces, start):
    first_k, second_k, value_rows = pieces
    length = first_k.shape[0]
    kv_local = first_q.shape[1]
    value_dim = value_rows.shape[1] // kv_local
    span = math.gcd(length, 2048)

    def sweep(current):

        def visit(block, inner):
            begin = block * span
            key_one = lax.dynamic_slice_in_dim(first_k, begin, span, 0).reshape(
                span, kv_local, HEAD
            )
            key_two = lax.dynamic_slice_in_dim(second_k, begin, span, 0).reshape(
                span, kv_local, HEAD
            )
            value_part = lax.dynamic_slice_in_dim(value_rows, begin, span, 0).reshape(
                span, kv_local, value_dim
            )
            key_pos = begin + jnp.arange(span, dtype=jnp.int32)
            return absorb(
                inner, first_q, second_q, key_one, key_two, value_part, query_pos, key_pos
            )

        return lax.fori_loop(0, length // span, visit, current)

    def unchanged(current):
        return current

    return lax.cond(start <= last_row, sweep, unchanged, state)


def finish_heads(final, head_lambda):
    kv_local, group, count, value_dim = final[2].shape
    weight = head_lambda.reshape(kv_local, group, 1, 1)
    head_out = final[2] / final[1][..., None] - weight * final[5] / final[4][..., None]
    head_out = head_out * lax.rsqrt(jnp.mean(head_out * head_out, axis=-1, keepdims=True) + 1e-05)
    return (
        head_out.transpose(2, 0, 1, 3)
        .reshape(count, kv_local * group * value_dim)
        .astype(jnp.bfloat16)
    )


def shared_part(normed, s_gate, s_up, s_down):
    piece = lax.all_gather(normed, "tp", axis=0, tiled=True)
    gate_part = jnp.dot(piece, s_gate, preferred_element_type=jnp.float32)
    up_part = jnp.dot(piece, s_up, preferred_element_type=jnp.float32)
    hidden = (jax.nn.silu(gate_part) * up_part).astype(jnp.bfloat16)
    terms = jnp.dot(hidden, s_down, preferred_element_type=jnp.float32)
    return lax.psum_scatter(
        terms.astype(jnp.bfloat16), "tp", scatter_dimension=0, tiled=True
    ).astype(jnp.float32)


def routed_part(normed, routes, route_w, w_gate, w_up, w_down):
    rows, topk = routes.shape
    local_experts = w_gate.shape[0]
    experts = local_experts * lax.axis_size("sp")
    slots = max(2, 3 * rows * topk // (2 * experts))
    flat_ids = routes.reshape(-1)
    hits = (flat_ids[:, None] == jnp.arange(experts, dtype=jnp.int32)[None, :]).astype(jnp.int32)
    slot_of = jnp.sum(jnp.cumsum(hits, axis=0) * hits, axis=1) - 1
    target = flat_ids * slots + slot_of
    placing = jnp.any(
        jnp.arange(experts * slots, dtype=jnp.int32)[:, None, None]
        == target.reshape(rows, topk)[None, :, :],
        axis=-1,
    ).astype(jnp.bfloat16)
    outgoing = (
        jnp.dot(placing, normed, preferred_element_type=jnp.float32)
        .astype(jnp.bfloat16)
        .reshape(experts, slots, normed.shape[1])
    )
    arrived = lax.all_to_all(outgoing, "sp", split_axis=0, concat_axis=0, tiled=True)
    sources = arrived.shape[0] // local_experts
    grouped = arrived.reshape(sources, local_experts, arrived.shape[1], arrived.shape[2])
    gate_part = jnp.einsum("sjcd,jdf->sjcf", grouped, w_gate, preferred_element_type=jnp.float32)
    up_part = jnp.einsum("sjcd,jdf->sjcf", grouped, w_up, preferred_element_type=jnp.float32)
    hidden = (jax.nn.silu(gate_part) * up_part).astype(jnp.bfloat16)
    result = jnp.einsum(
        "sjcf,jfd->sjcd", hidden, w_down, preferred_element_type=jnp.float32
    ).astype(jnp.bfloat16)
    returned = lax.all_to_all(
        result.reshape(arrived.shape), "sp", split_axis=0, concat_axis=0, tiled=True
    )
    picked = (
        returned.reshape(experts * slots, normed.shape[1])[target]
        .reshape(rows, topk, normed.shape[1])
        .astype(jnp.float32)
    )
    return jnp.sum(picked * route_w[..., None], axis=1)


def local(
    stream_in,
    q_first,
    q_second,
    k_first,
    k_second,
    values,
    head_lambda,
    w_out,
    norm_gain,
    routes,
    route_w,
    w_gate,
    w_up,
    w_down,
    s_gate,
    s_up,
    s_down,
):
    seq_rows = q_first.shape[0]
    kv_local = k_first.shape[1] // HEAD
    heads_local = q_first.shape[1] // HEAD
    group = heads_local // kv_local
    value_dim = values.shape[1] // kv_local
    offset = lax.axis_index("sp") * seq_rows
    query_pos = offset + jnp.arange(seq_rows, dtype=jnp.int32)
    last_row = offset + seq_rows - 1
    first_q = q_first.reshape(seq_rows, kv_local, group, HEAD)
    second_q = q_second.reshape(seq_rows, kv_local, group, HEAD)
    start_state = empty_state(kv_local, group, seq_rows, value_dim)
    folded_state = fold_rows(
        start_state,
        first_q,
        second_q,
        query_pos,
        last_row,
        side_by_side((k_first, k_second, values), "sp", 0, 1),
        jnp.int32(0),
    )
    attn_rows = finish_heads(folded_state, head_lambda)
    attn = sum_at_owner(
        jnp.dot(attn_rows, w_out, preferred_element_type=jnp.float32).astype(jnp.bfloat16), "tp", 0
    )
    resid = (stream_in.astype(jnp.float32) + attn).astype(jnp.bfloat16)
    stream = lax.optimization_barrier(resid).astype(jnp.float32)
    normed = (
        stream * lax.rsqrt(jnp.mean(stream * stream, axis=-1, keepdims=True) + 1e-06) * norm_gain
    ).astype(jnp.bfloat16)
    routed = routed_part(normed, routes, route_w, w_gate, w_up, w_down)
    shared = shared_part(normed, s_gate, s_up, s_down)
    return (stream + routed + shared).astype(jnp.bfloat16)


def solution(mesh):
    return jax.shard_map(
        local,
        mesh=mesh,
        in_specs=(
            P(("sp", "tp"), None),
            P("sp", "tp"),
            P("sp", "tp"),
            P("sp", "tp"),
            P("sp", "tp"),
            P("sp", "tp"),
            P("tp"),
            P("tp", None),
            P(),
            P(("sp", "tp"), None),
            P(("sp", "tp"), None),
            P("sp", None, None),
            P("sp", None, None),
            P("sp", None, None),
            P(None, "tp"),
            P(None, "tp"),
            P("tp", None),
        ),
        out_specs=P(("sp", "tp"), None),
        check_vma=False,
    )
```

profile of v0, /device:TPU:8, one launch (start us, length us, event | category | flops | bytes accessed | tf_op | source)
XLA Modules:
  0.0 570.8 jit_solution(7745764159764571665)
XLA Ops:
  8.3 102.7 %all-gather.3.cloned.1.call-done = bf16[16384,512]{1,0:T(8,128)(2,1)} async-done(((bf16[256,512]{1,0:T(8,128)(2,1)}), bf16[16384,512]{1,0:T(8,128)(2,1)}) %all-gather.3.cloned.1.call-update) | async-done | bytes 16777232 | tf_op jit(solution)/shard_map/all_gather | solution.py:17
  111.0 158.4 %conditional.1 = (f32[1,2,256]{2,1,0:T(2,128)}, f32[1,2,256]{2,1,0:T(2,128)}, f32[1,2,256,256]{2,3,1,0:T(8,128)S(1)}, f32[1,2,256,256]{2,3,1,0:T(8,128)S(1)}) conditional(s32[]{:T(128)} %convert_element_type.81, () %tuple.27, (bf16[16384,512]{1,0:T(8,128)(2,1)}, s32[]{:T(128)}, s32[256]{0:T(256)S(1)}, bf16[256,256]{1,0:T(8,128)(2,1)}, ...), branch_computations={%region_0.0_spmd, %region_1.8_spmd} | conditional | flops 1639194880 | bytes 192761424 | solution.py:97
  111.0 6.8 %fusion.100 = (bf16[16384,128]{1,0:T(8,128)(2,1)}, bf16[16384,128]{1,0:T(8,128)(2,1)}) fusion(bf16[16384,512]{1,0:T(8,128)(2,1)} %get-tuple-element.239), kind=kLoop, calls=%fused_computation.124 | loop fusion | bytes 16777216 | tf_op jit(solution)/shard_map/split | solution.py:18
  126.3 142.6 %while.23 = (s32[]{:T(128)}, f32[1,2,256]{2,1,0:T(2,128)S(1)}, f32[1,2,256]{2,1,0:T(2,128)}, f32[1,2,256,256]{3,2,1,0:T(8,128)S(1)}, f32[1,2,256]{2,1,0:T(2,128)...) while((s32[]{:T(128)}, f32[1,2,256]{2,1,0:T(2,128)S(1)}, ...), condition=%wide.region_7.7_spmd.clone, body=%wide.region_2.6_spmd.clone.sunk | while | flops 1639194624 | bytes 87901504 | solution.py:92
  128.6 4.9 fusion.131
  145.8 4.9 fusion.131
  163.8 4.9 fusion.131
  181.7 4.9 fusion.131
  199.6 4.9 fusion.131
  217.5 4.9 fusion.131
  235.4 4.9 fusion.131
  253.3 4.9 fusion.131
  281.0 25.1 %all-to-all-done = bf16[4,64,4096]{2,1,0:T(8,128)(2,1)S(1)} async-done(((bf16[4,64,4096]{2,1,0:T(8,128)(2,1)}), bf16[4,64,4096]{2,1,0:T(8,128)(2,1)S(1)}, u32[]{:S(2)}, u32[]{:S(2)}) %all-to-all-start) | async-done | bytes 2097184 | tf_op jit(solution)/shard_map/all_to_all | solution.py:29
  311.3 5.7 reshape.229
  317.0 7.9 %all-to-all-start.1 = ((bf16[64,6,4096]{2,1,0:T(8,128)(2,1)}), bf16[64,6,4096]{2,1,0:T(8,128)(2,1)}, u32[]{:S(2)}, u32[]{:S(2)}) async-start(bf16[64,6,4096]{2,1,0:T(8,128)(2,1)} %reshape.229), calls=%async_computation.1 | async-start | bytes 8388608 | tf_op jit(solution)/shard_map/all_to_all | solution.py:142
  325.7 95.3 %all-to-all-done.1 = bf16[64,6,4096]{2,1,0:T(8,128)(2,1)} async-done(((bf16[64,6,4096]{2,1,0:T(8,128)(2,1)}), bf16[64,6,4096]{2,1,0:T(8,128)(2,1)}, u32[]{:S(2)}, u32[]{:S(2)}) %all-to-all-start.1) | async-done | bytes 3145760 | tf_op jit(solution)/shard_map/all_to_all | solution.py:142
  421.0 5.9 %fusion.54 = f32[64,1,6,128]{3,0,2,1:T(8,128)S(1)} fusion(bf16[64,6,4096]{2,1,0:T(8,128)(2,1)} %all-to-all-done.1, bf16[1,4096,128]{2,1,0:T(8,128)(2,1)} %param.32), kind=kOutput, calls=%fused_computation.73 | convolution fusion | flops 402653184 | bytes 4390912 | tf_op jit(solution)/shard_map/sjcd,jdf->sjcf/dot_general | solution.py:145
  426.9 7.4 %convolution_convert_fusion.1 = bf16[64,6,4096]{2,0,1:T(8,128)(2,1)} fusion(bf16[64,6,4096]{2,1,0:T(8,128)(2,1)} %all-to-all-done.1, bf16[1,128,4096]{2,1,0:T(8,128)(2,1)S(1)} %copy-done, bf16[1,4096,128]{2,1,0:T(8,128)(2,1)S(1)} %copy-done.9, f32[64,1,6,128]{3,0,2,1:T(8,128)S(1)} %fusion.54), kind=kOutput, calls=%fused_computation.61 | convolution fusion | flops 807174144 | bytes 8585216 | tf_op jit(solution)/shard_map/sjcf,jfd->sjcd/dot_general | solution.py:148
  434.4 5.6 copy.71
  440.0 5.7 all-to-all-start.2
  453.2 88.7 %all-to-all-done.2 = bf16[64,6,4096]{2,1,0:T(8,128)(2,1)} async-done(((bf16[64,6,4096]{2,1,0:T(8,128)(2,1)}), bf16[64,6,4096]{2,1,0:T(8,128)(2,1)}, u32[]{:S(2)}, u32[]{:S(2)}) %all-to-all-start.2) | async-done | bytes 3145760 | tf_op jit(solution)/shard_map/all_to_all | solution.py:151
  541.9 5.7 %reshape.234 = bf16[384,4096]{1,0:T(8,128)(2,1)} reshape(bf16[64,6,4096]{2,1,0:T(8,128)(2,1)} %all-to-all-done.2) | data formatting | bytes 6291456 | tf_op jit(solution)/shard_map/reshape | solution.py:155
  547.6 6.2 %gather_fusion = bf16[256,4096]{1,0:T(8,128)(2,1)S(1)} fusion(bf16[384,4096]{1,0:T(8,128)(2,1)} %reshape.234, s32[1024]{0:T(1024)S(1)} %pad_clamp_fusion), kind=kCustom, calls=%fused_computation | custom fusion | bytes 4195328 | tf_op jit(solution)/shard_map/gather | solution.py:155
  556.9 5.3 multiply_reduce_fusion
  (219 shorter events, 143.2 us)
Async XLA Ops:
  6.5 420.4 %copy-start = (bf16[1,128,4096]{2,1,0:T(8,128)(2,1)S(1)}, bf16[1,128,4096]{2,1,0:T(8,128)(2,1)}, u32[]{:S(2)}) copy-start(bf16[1,128,4096]{2,1,0:T(8,128)(2,1)} %param.34) | copy-start | bytes 3145732
  6.5 104.5 %all-gather.3.cloned.1.call-start = ((), (), s32[]{:S(2)}) async-start(), calls=%async_computation.4 | async-start | bytes 17039360 | tf_op jit(solution)/shard_map/all_gather | solution.py:17
  111.0 158.4 %copy-start.15 = (f32[2]{0:T(128)S(1)}, f32[2]{0:T(128)}, u32[]{:S(2)}) copy-start(f32[2]{0:T(128)} %param.27) | copy-start | bytes 28
  111.0 11.2 %copy-start.4 = (bf16[16384,512]{1,0:T(8,128)(2,1)S(1)}, bf16[16384,512]{1,0:T(8,128)(2,1)}, u32[]{:S(2)}) copy-start(bf16[16384,512]{1,0:T(8,128)(2,1)} %get-tuple-element.239) | copy-start | bytes 50331652 | tf_op jit(solution)/shard_map/cond
  128.1 5.4 copy-start.1
  133.5 4.3 copy-start.2
  145.3 5.4 copy-start.1
  163.3 5.4 copy-start.1
  181.2 5.4 copy-start.1
  199.1 5.4 copy-start.1
  217.0 5.4 copy-start.1
  234.9 5.4 copy-start.1
  252.8 5.4 copy-start.1
  270.3 9.1 %copy-start.13 = (s32[64,4]{0,1:T(4,128)S(1)}, s32[64,4]{0,1:T(4,128)}, u32[]{:S(2)}) copy-start(s32[64,4]{0,1:T(4,128)} %param.30) | copy-start | bytes 3076
  275.2 31.0 %all-to-all-start = ((bf16[4,64,4096]{2,1,0:T(8,128)(2,1)}), bf16[4,64,4096]{2,1,0:T(8,128)(2,1)S(1)}, u32[]{:S(2)}, u32[]{:S(2)}) async-start(bf16[4,64,4096]{2,1,0:T(8,128)(2,1)} %bitcast.6), calls=%async_computation | async-start | bytes 4194304 | tf_op jit(solution)/shard_map/all_to_all | solution.py:29
  279.4 29.0 %copy-start.12 = (f32[4096]{0:T(1024)S(1)}, f32[4096]{0:T(1024)}, u32[]{:S(2)}) copy-start(f32[4096]{0:T(1024)} %param.29) | copy-start | bytes 49156
  308.6 8.4 %copy-start.8 = (bf16[64,4096]{1,0:T(8,128)(2,1)}, bf16[64,4096]{1,0:T(8,128)(2,1)S(1)}, u32[]{:S(2)}) copy-start(bf16[64,4096]{1,0:T(8,128)(2,1)S(1)} %fusion.74) | copy-start | bytes 1572868
  317.0 104.0 %all-to-all-start.1 = ((bf16[64,6,4096]{2,1,0:T(8,128)(2,1)}), bf16[64,6,4096]{2,1,0:T(8,128)(2,1)}, u32[]{:S(2)}, u32[]{:S(2)}) async-start(bf16[64,6,4096]{2,1,0:T(8,128)(2,1)} %reshape.229), calls=%async_computation.1 | async-start | bytes 8388608 | tf_op jit(solution)/shard_map/all_to_all | solution.py:142
  324.9 102.0 %copy-start.9 = (bf16[1,4096,128]{2,1,0:T(8,128)(2,1)S(1)}, bf16[1,4096,128]{2,1,0:T(8,128)(2,1)}, u32[]{:S(2)}) copy-start(bf16[1,4096,128]{2,1,0:T(8,128)(2,1)} %param.33) | copy-start | bytes 3145732
  324.9 121.1 %all-gather.5.cloned.1.call-start = ((), (), s32[]{:S(2)}) async-start(), calls=%async_computation.5 | async-start | bytes 2621440 | tf_op jit(solution)/shard_map/all_gather | solution.py:113
  440.0 101.9 %all-to-all-start.2 = ((bf16[64,6,4096]{2,1,0:T(8,128)(2,1)}), bf16[64,6,4096]{2,1,0:T(8,128)(2,1)}, u32[]{:S(2)}, u32[]{:S(2)}) async-start(bf16[64,6,4096]{2,1,0:T(8,128)(2,1)} %copy.71), calls=%async_computation.2 | async-start | bytes 8388608 | tf_op jit(solution)/shard_map/all_to_all | solution.py:151
  445.7 116.5 %reduce-scatter.2.cloned.1.call-start = ((), (), s32[]{:S(2)}) async-start(), calls=%async_computation.6 | async-start | bytes 2621440 | tf_op jit(solution)/shard_map/reduce_scatter | solution.py:118
  448.7 4.4 copy-start.14
  556.9 5.4 copy-start.7
  (19 other events, 65.3 us)
Sparse Core Ops, SparseCore 0:
  10.1 100.8 all-gather.2
  327.6 32.5 all-gather.4
  453.1 31.5 reduce-scatter.1
where the time goes:
time: 572 us; the launch traced here: 571 us
  waiting for transfers between devices  313 us (55%)
  matrix products  139 us (24%)
  local copies, waits for them, and re-layouts  43.5 us (8%)
  other arithmetic  43.1 us (8%)
  starting transfers between devices  18.2 us (3%)
  between operations  13.4 us (2%)
    all_gather x1, waiting for transfers between devices, side_by_side(): out = lax.all_gather(both, axis, axis=dim, tiled=True)  103 us
    all_to_all x1, waiting for transfers between devices, routed_part(): lax.all_to_all(outgoing, 'sp', split_axis=0, concat_axis=0, tiled=True)  95.3 us
    all_to_all x1, waiting for transfers between devices, routed_part(): lax.all_to_all(result.reshape(arrived.shape), 'sp', split_axis=0, concat_...  88.7 us
    dot_general x16, matrix products, absorb(): jnp.einsum('agqk,kad->agqd', weights.astype(jnp.bfloat16), value_rows, pr...  58.2 us
    dot_general x16, matrix products, absorb(): jnp.einsum('qagd,kad->agqk', query_rows, key_rows, preferred_element_type...  53.3 us
    all_to_all x1, waiting for transfers between devices, sum_at_owner(): pieces = lax.all_to_all(cut_along(x, dim, count), axis, 0, 0, tiled=True)  25.1 us
    reduce_sum x8, other arithmetic, absorb(): total = total * fade + weights.sum(-1)  16.7 us
  transfers between devices with their start and end apart: 6, of which 4 were waited for; matrix products, arithmetic and copies ran while one was open for 8% of the time, Pallas kernels for 0%

commit v1 on v0

v1 whole, which is shorter than its diff:
```python
import functools
import math

import jax
import jax.numpy as jnp
from jax import lax
from jax.experimental import pallas as pl
from jax.experimental.pallas import tpu as pltpu
from jax.sharding import PartitionSpec as P

HEAD = 128
VD = 256
FLOOR = -1e30
NZ = 8
NY = 4
NCHIP = NZ * NY
BLK = 256
PAIR = 2 * BLK
KVW = 512
LOG2E = 1.4426950408889634

ORDER = sorted(
    [(dz, dy) for dz in (0, 1, -1, 2, -2, 3, -3, 4) for dy in (0, 1, -1, 2)],
    key=lambda a: (abs(a[0]) + abs(a[1]), -abs(a[0]), a),
)
PIECES = ((0, 80, "z", 1), (80, 80, "z", -1), (160, 48, "y", 1), (208, 48, "y", -1))


def step_counts():
    sent = {"z+": 0, "z-": 0, "y+": 0, "y-": 0}
    for dz, dy in ORDER:
        for _, rows, first, way in PIECES:
            for link, go in hops(dz, dy, first, way).items():
                if go:
                    sent[link] += rows
    return sent


def hops(dz, dy, first, way):
    zup = (dz >= 0) & (dz < (4 if way > 0 else 3))
    zdown = (dz <= 0) & (dz > (-3 if way > 0 else -4))
    yup = (dy >= 0) & (dy < (2 if way > 0 else 1))
    ydown = (dy <= 0) & (dy > (-1 if way > 0 else -2))
    if first == "z":
        zup, zdown = zup & (dy == 0), zdown & (dy == 0)
    else:
        yup, ydown = yup & (dz == 0), ydown & (dz == 0)
    return {"z+": zup, "z-": zdown, "y+": yup, "y-": ydown}


def lookup(values, index):
    out = jnp.int32(values[0])
    for k, v in enumerate(values[1:], 1):
        out = jnp.where(index == k, jnp.int32(v), out)
    return out


def attn_kernel(
    lam_ref, q1_ref, q2_ref, k1_hbm, k2_hbm, v_hbm, out_ref,
    kv, q_s, m_s, l_s, acc_s, load_sem, send_sem, recv_sem, pair_sem,
):
    me = lax.axis_index("sp")
    c = me % 2
    y = (me // 2) % NY
    z = me // (2 * NY)
    chip = z * NY + y

    def at(zz, yy, cc):
        return {"sp": ((zz + NZ) % NZ) * (2 * NY) + ((yy + NY) % NY) * 2 + cc}

    peers = {
        "z+": at(z + 1, y, c), "z-": at(z - 1, y, c),
        "y+": at(z, y + 1, c), "y-": at(z, y - 1, c),
        "pair": at(z, y, 1 - c),
    }
    links = ("z+", "z-", "y+", "y-", "pair")

    own = pl.multiple_of(chip * PAIR + c * BLK, BLK)
    loads = []
    for k, (src, lo, hi) in enumerate(((k1_hbm, 0, 128), (k2_hbm, 128, 256), (v_hbm, 256, 512))):
        loads.append(pltpu.make_async_copy(src, kv.at[pl.ds(own, BLK), lo:hi], load_sem.at[k]))
        loads[-1].start()

    barrier = pltpu.get_barrier_semaphore()
    for link in links:
        pl.semaphore_signal(barrier, inc=1, device_id=peers[link], device_id_type=pl.DeviceIdType.MESH)

    scale = HEAD ** (-0.5) * LOG2E
    for k, ref in enumerate((q1_ref, q2_ref)):
        for h in range(2):
            q_s[k, h * BLK : (h + 1) * BLK, :] = ref[:, h * HEAD : (h + 1) * HEAD]
    m_s[...] = jnp.full_like(m_s, FLOOR)
    l_s[...] = jnp.zeros_like(l_s)
    acc_s[...] = jnp.zeros_like(acc_s)

    pl.semaphore_wait(barrier, len(links))
    for copy in loads:
        copy.wait()

    def rows_of(src_chip, core, first, rows):
        return kv.at[pl.ds(pl.multiple_of(src_chip * PAIR + core * BLK + first, 16), rows), :]

    def remote(ref, link, sem):
        return pltpu.make_async_remote_copy(
            src_ref=ref, dst_ref=ref, send_sem=send_sem.at[links.index(link)], recv_sem=sem,
            device_id=peers[link], device_id_type=pl.DeviceIdType.MESH,
        )

    def forward(dz, dy, src_chip):
        for first_row, rows, first, way in PIECES:
            for link, go in hops(dz, dy, first, way).items():

                @pl.when(go)
                def _():
                    remote(rows_of(src_chip, c, first_row, rows), link, recv_sem.at[src_chip]).start()

        remote(rows_of(src_chip, c, 0, BLK), "pair", pair_sem.at[src_chip]).start()

    def attend(src_chip, masked):
        base = pl.multiple_of(src_chip * PAIR, PAIR)
        value = kv[pl.ds(base, PAIR), 256:512]
        for k in range(2):
            key = kv[pl.ds(base, PAIR), k * HEAD : (k + 1) * HEAD]
            scores = lax.dot_general(
                q_s[k], key, (((1,), (1,)), ((), ())), preferred_element_type=jnp.float32
            ) * scale
            if masked:
                q_pos = lax.broadcasted_iota(jnp.int32, scores.shape, 0) % BLK + c * BLK
                k_pos = lax.broadcasted_iota(jnp.int32, scores.shape, 1)
                scores = jnp.where(k_pos <= q_pos, scores, FLOOR)
            old = m_s[k]
            new = jnp.maximum(old, jnp.max(scores, axis=1, keepdims=True))
            fade = jnp.exp2(old - new)
            weights = jnp.exp2(scores - jnp.tile(new, (1, PAIR // 128)))
            if masked:
                weights = jnp.where(k_pos <= q_pos, weights, 0.0)
            part = weights[:, 0:128]
            for t in range(1, PAIR // 128):
                part = part + weights[:, t * 128 : (t + 1) * 128]
            m_s[k] = new
            l_s[k] = l_s[k] * fade + part
            acc_s[k] = acc_s[k] * jnp.tile(fade, (1, VD // 128)) + jnp.dot(
                weights.astype(jnp.bfloat16), value, preferred_element_type=jnp.float32
            )

    forward(jnp.int32(0), jnp.int32(0), chip)

    dz_table = [o[0] for o in ORDER]
    dy_table = [o[1] for o in ORDER]

    def place(e):
        dz, dy = lookup(dz_table, e), lookup(dy_table, e)
        return dz, dy, ((z - dz + NZ) % NZ) * NY + (y - dy + NY) % NY

    def step(e, carry):
        @pl.when(e < NCHIP)
        def _():
            dz, dy, src = place(e)
            remote(rows_of(src, c, 0, BLK), "z+", recv_sem.at[src]).wait_recv()
            forward(dz, dy, src)

        _, _, last = place(e - 1)
        remote(rows_of(last, 1 - c, 0, BLK), "pair", pair_sem.at[last]).wait_recv()

        @pl.when(e == 1)
        def _():
            attend(chip, True)

        @pl.when((e > 1) & (last < chip))
        def _():
            attend(last, False)

        return carry

    lax.fori_loop(1, NCHIP + 1, step, 0)

    head_rows = []
    for k in range(2):
        total = jnp.sum(l_s[k], axis=1, keepdims=True)
        head_rows.append(acc_s[k] / total)
    for h in range(2):
        span = slice(h * BLK, (h + 1) * BLK)
        head = head_rows[0][span] - lam_ref[h] * head_rows[1][span]
        head = head * lax.rsqrt(jnp.mean(head * head, axis=1, keepdims=True) + 1e-05)
        out_ref[:, h * VD : (h + 1) * VD] = head.astype(jnp.bfloat16)

    for link, rows in step_counts().items():
        remote(kv.at[pl.ds(0, rows), :], link, recv_sem.at[0]).wait_send()
    remote(kv.at[pl.ds(0, NCHIP * BLK), :], "pair", recv_sem.at[0]).wait_send()


def attention(head_lambda, q_first, q_second, k_first, k_second, values):
    vmem = pl.BlockSpec(memory_space=pltpu.VMEM)
    hbm = pl.BlockSpec(memory_space=pl.ANY)
    return pl.pallas_call(
        attn_kernel,
        out_shape=jax.ShapeDtypeStruct((BLK, 2 * VD), jnp.bfloat16),
        in_specs=[pl.BlockSpec(memory_space=pltpu.SMEM), vmem, vmem, hbm, hbm, hbm],
        out_specs=vmem,
        scratch_shapes=[
            pltpu.VMEM((NCHIP * PAIR, KVW), jnp.bfloat16),
            pltpu.VMEM((2, 2 * BLK, HEAD), jnp.bfloat16),
            pltpu.VMEM((2, 2 * BLK, 128), jnp.float32),
            pltpu.VMEM((2, 2 * BLK, 128), jnp.float32),
            pltpu.VMEM((2, 2 * BLK, VD), jnp.float32),
            pltpu.SemaphoreType.DMA((3,)),
            pltpu.SemaphoreType.DMA((5,)),
            pltpu.SemaphoreType.DMA((NCHIP,)),
            pltpu.SemaphoreType.DMA((NCHIP,)),
        ],
        compiler_params=pltpu.CompilerParams(
            collective_id=0, has_side_effects=True, vmem_limit_bytes=48 * 1024 * 1024
        ),
        name="attend",
    )(head_lambda, q_first, q_second, k_first, k_second, values)


def cut_along(x, dim, count):
    shape = x.shape
    pieces = x.reshape(*shape[:dim], count, shape[dim] // count, *shape[dim + 1 :])
    return jnp.moveaxis(pieces, dim, 0)


def sum_at_owner(x, axis, dim):
    count = lax.axis_size(axis)
    pieces = lax.all_to_all(cut_along(x, dim, count), axis, 0, 0, tiled=True)
    return jnp.sum(pieces.astype(jnp.float32), axis=0)


def shared_part(normed, s_gate, s_up, s_down):
    piece = lax.all_gather(normed, "tp", axis=0, tiled=True)
    gate_part = jnp.dot(piece, s_gate, preferred_element_type=jnp.float32)
    up_part = jnp.dot(piece, s_up, preferred_element_type=jnp.float32)
    hidden = (jax.nn.silu(gate_part) * up_part).astype(jnp.bfloat16)
    terms = jnp.dot(hidden, s_down, preferred_element_type=jnp.float32)
    return lax.psum_scatter(
        terms.astype(jnp.bfloat16), "tp", scatter_dimension=0, tiled=True
    ).astype(jnp.float32)


def routed_part(normed, routes, route_w, w_gate, w_up, w_down):
    rows, topk = routes.shape
    local_experts = w_gate.shape[0]
    experts = local_experts * lax.axis_size("sp")
    slots = max(2, 3 * rows * topk // (2 * experts))
    flat_ids = routes.reshape(-1)
    hits = (flat_ids[:, None] == jnp.arange(experts, dtype=jnp.int32)[None, :]).astype(jnp.int32)
    slot_of = jnp.sum(jnp.cumsum(hits, axis=0) * hits, axis=1) - 1
    target = flat_ids * slots + slot_of
    placing = jnp.any(
        jnp.arange(experts * slots, dtype=jnp.int32)[:, None, None]
        == target.reshape(rows, topk)[None, :, :],
        axis=-1,
    ).astype(jnp.bfloat16)
    outgoing = (
        jnp.dot(placing, normed, preferred_element_type=jnp.float32)
        .astype(jnp.bfloat16)
        .reshape(experts, slots, normed.shape[1])
    )
    arrived = lax.all_to_all(outgoing, "sp", split_axis=0, concat_axis=0, tiled=True)
    sources = arrived.shape[0] // local_experts
    grouped = arrived.reshape(sources, local_experts, arrived.shape[1], arrived.shape[2])
    gate_part = jnp.einsum("sjcd,jdf->sjcf", grouped, w_gate, preferred_element_type=jnp.float32)
    up_part = jnp.einsum("sjcd,jdf->sjcf", grouped, w_up, preferred_element_type=jnp.float32)
    hidden = (jax.nn.silu(gate_part) * up_part).astype(jnp.bfloat16)
    result = jnp.einsum(
        "sjcf,jfd->sjcd", hidden, w_down, preferred_element_type=jnp.float32
    ).astype(jnp.bfloat16)
    returned = lax.all_to_all(
        result.reshape(arrived.shape), "sp", split_axis=0, concat_axis=0, tiled=True
    )
    picked = (
        returned.reshape(experts * slots, normed.shape[1])[target]
        .reshape(rows, topk, normed.shape[1])
        .astype(jnp.float32)
    )
    return jnp.sum(picked * route_w[..., None], axis=1)


def local(
    stream_in,
    q_first,
    q_second,
    k_first,
    k_second,
    values,
    head_lambda,
    w_out,
    norm_gain,
    routes,
    route_w,
    w_gate,
    w_up,
    w_down,
    s_gate,
    s_up,
    s_down,
):
    attn_rows = attention(head_lambda, q_first, q_second, k_first, k_second, values)
    attn = sum_at_owner(
        jnp.dot(attn_rows, w_out, preferred_element_type=jnp.float32).astype(jnp.bfloat16), "tp", 0
    )
    resid = (stream_in.astype(jnp.float32) + attn).astype(jnp.bfloat16)
    stream = lax.optimization_barrier(resid).astype(jnp.float32)
    normed = (
        stream * lax.rsqrt(jnp.mean(stream * stream, axis=-1, keepdims=True) + 1e-06) * norm_gain
    ).astype(jnp.bfloat16)
    routed = routed_part(normed, routes, route_w, w_gate, w_up, w_down)
    shared = shared_part(normed, s_gate, s_up, s_down)
    return (stream + routed + shared).astype(jnp.bfloat16)


def solution(mesh):
    return jax.shard_map(
        local,
        mesh=mesh,
        in_specs=(
            P(("sp", "tp"), None),
            P("sp", "tp"),
            P("sp", "tp"),
            P("sp", "tp"),
            P("sp", "tp"),
            P("sp", "tp"),
            P("tp"),
            P("tp", None),
            P(),
            P(("sp", "tp"), None),
            P(("sp", "tp"), None),
            P("sp", None, None),
            P("sp", None, None),
            P("sp", None, None),
            P(None, "tp"),
            P(None, "tp"),
            P("tp", None),
        ),
        out_specs=P(("sp", "tp"), None),
        check_vma=False,
    )
```

time: 572 us -> 375 us (0.66)
  matrix products: 139 us -> 27.7 us
  waiting for transfers between devices: 313 us -> 210 us
  Pallas kernels: 0 us -> 61.5 us
  other arithmetic: 43.1 us -> 9.07 us
  local copies, waits for them, and re-layouts: 43.5 us -> 33.6 us
    dot_general x32 -> x0, matrix products: 112 us -> none  [the longest x16 58.2 us: absorb(): jnp.einsum('agqk,kad->agqd', weights.astype(jnp.bfloat16), value_rows, pr...]
    all_gather x1 -> x0, waiting for transfers between devices: 103 us -> none  [side_by_side(): out = lax.all_gather(both, axis, axis=dim, tiled=True)]
    pallas_call x0 -> x1, Pallas kernels: none -> 61.5 us  [attention(): pl.pallas_call(attn_kernel, out_shape=jax.ShapeDtypeStruct((BLK, 2 * VD),...]
    reduce_sum x9 -> x0, other arithmetic: 17.6 us -> none  [the longest x8 16.7 us: absorb(): total = total * fade + weights.sum(-1)]
    split x2 -> x0, local copies, waits for them, and re-layouts: 10.4 us -> none  [side_by_side(): jnp.split(out, [sum(widths[:k]) for k in range(1, len(widths))], axis=along)]
    add x17 -> x0, other arithmetic: 9.66 us -> none  [the longest x8 9.62 us: absorb(): total = total * fade + weights.sum(-1)]
    unnamed x22 -> x34, local copies, waits for them, and re-layouts: 0.8 us -> 6.65 us
  transfers between devices with their start and end apart: 6 -> 5, of which waited for: 4 -> 3; matrix products, arithmetic and copies ran while one was open for 8% -> 13% of each run, Pallas kernels for 0% -> 0%
where the time goes in v1:
time: 375 us; the launch traced here: 374 us
  waiting for transfers between devices  210 us (56%)
  Pallas kernels  61.5 us (16%)
  local copies, waits for them, and re-layouts  33.6 us (9%)
  matrix products  27.7 us (7%)
  starting transfers between devices  18 us (5%)
  between operations  13.6 us (4%)
  other arithmetic  9.07 us (2%)
    all_to_all x1, waiting for transfers between devices, routed_part(): lax.all_to_all(outgoing, 'sp', split_axis=0, concat_axis=0, tiled=True)  95.3 us
    all_to_all x1, waiting for transfers between devices, routed_part(): lax.all_to_all(result.reshape(arrived.shape), 'sp', split_axis=0, concat_...  88.7 us
    pallas_call x1, Pallas kernels, attention(): pl.pallas_call(attn_kernel, out_shape=jax.ShapeDtypeStruct((BLK, 2 * VD),...  61.5 us
    all_to_all x1, waiting for transfers between devices, sum_at_owner(): pieces = lax.all_to_all(cut_along(x, dim, count), axis, 0, 0, tiled=True)  25.6 us
  transfers between devices with their start and end apart: 5, of which 3 were waited for; matrix products, arithmetic and copies ran while one was open for 13% of the time, Pallas kernels for 0%

profile of v1, /device:TPU:8, one launch (start us, length us, event | category | flops | bytes accessed | tf_op | source)
XLA Modules:
  0.0 373.6 jit_solution(14990297353015015769)
XLA Ops:
  6.5 1.0 copy-done.1
  7.5 0.9 copy-done.2
  8.4 0.9 copy-done.3
  9.3 0.8 copy-done.4
  11.7 61.5 %attend.1 = bf16[256,512]{1,0:T(8,128)(2,1)S(1)} custom-call(f32[2]{0:T(128)S(1)} %copy-done.6, bf16[256,256]{1,0:T(8,128)(2,1)S(1)} %copy-done.1, bf16[256,256]{1,0:T(8,128)(2,1)S(1)} %copy-done.2, bf16[256,128]{1,0:T(8,128)(2,1)S(1)} %copy-done.4, bf16[256,128]{1,0:T(8,128)(2,1)S(1)} %copy-done.5, bf16[256,256]{1,0:T(8,128)(2,1)S(1)} %copy-done.3), custom_call_target="tpu_custom_call" | custom-call | tf_op jit(solution)/shard_map/attend/pallas_call | solution.py:195
  73.2 4.8 %convolution_convert_fusion.3 = bf16[256,4096]{1,0:T(8,128)(2,1)} fusion(bf16[256,512]{1,0:T(8,128)(2,1)S(1)} %attend.1, bf16[512,4096]{1,0:T(8,128)(2,1)} %param.24), kind=kOutput, calls=%fused_computation.4 | convolution fusion | flops 1074790400 | bytes 6553600 | tf_op jit(solution)/shard_map/dot_general | solution.py:301
  77.9 4.4 %all-to-all-start = ((bf16[4,64,4096]{2,1,0:T(8,128)(2,1)}), bf16[4,64,4096]{2,1,0:T(8,128)(2,1)S(1)}, u32[]{:S(2)}, u32[]{:S(2)}) async-start(bf16[4,64,4096]{2,1,0:T(8,128)(2,1)} %bitcast.64), calls=%async_computation | async-start | bytes 4194304 | tf_op jit(solution)/shard_map/all_to_all | solution.py:226
  84.0 25.6 %all-to-all-done = bf16[4,64,4096]{2,1,0:T(8,128)(2,1)S(1)} async-done(((bf16[4,64,4096]{2,1,0:T(8,128)(2,1)}), bf16[4,64,4096]{2,1,0:T(8,128)(2,1)S(1)}, u32[]{:S(2)}, u32[]{:S(2)}) %all-to-all-start) | async-done | bytes 2097184 | tf_op jit(solution)/shard_map/all_to_all | solution.py:226
  111.7 2.7 convolution_convert_fusion
  114.4 5.7 %reshape.106 = bf16[64,6,4096]{2,1,0:T(8,128)(2,1)} reshape(bf16[384,4096]{1,0:T(8,128)(2,1)} %convolution_convert_fusion) | data formatting | bytes 6291456 | tf_op jit(solution)/shard_map/reshape | solution.py:258
  120.1 7.4 %all-to-all-start.1 = ((bf16[64,6,4096]{2,1,0:T(8,128)(2,1)}), bf16[64,6,4096]{2,1,0:T(8,128)(2,1)}, u32[]{:S(2)}, u32[]{:S(2)}) async-start(bf16[64,6,4096]{2,1,0:T(8,128)(2,1)} %reshape.106), calls=%async_computation.1 | async-start | bytes 8388608 | tf_op jit(solution)/shard_map/all_to_all | solution.py:260
  128.2 95.3 %all-to-all-done.1 = bf16[64,6,4096]{2,1,0:T(8,128)(2,1)} async-done(((bf16[64,6,4096]{2,1,0:T(8,128)(2,1)}), bf16[64,6,4096]{2,1,0:T(8,128)(2,1)}, u32[]{:S(2)}, u32[]{:S(2)}) %all-to-all-start.1) | async-done | bytes 3145760 | tf_op jit(solution)/shard_map/all_to_all | solution.py:260
  223.6 5.9 %fusion.4 = f32[64,1,6,128]{3,0,2,1:T(8,128)S(1)} fusion(bf16[64,6,4096]{2,1,0:T(8,128)(2,1)} %all-to-all-done.1, bf16[1,4096,128]{2,1,0:T(8,128)(2,1)} %param.28), kind=kOutput, calls=%fused_computation.14 | convolution fusion | flops 402653184 | bytes 4390912 | tf_op jit(solution)/shard_map/sjcd,jdf->sjcf/dot_general | solution.py:263
  229.5 7.4 %convolution_convert_fusion.1 = bf16[64,6,4096]{2,0,1:T(8,128)(2,1)} fusion(bf16[64,6,4096]{2,1,0:T(8,128)(2,1)} %all-to-all-done.1, bf16[1,128,4096]{2,1,0:T(8,128)(2,1)S(1)} %copy-done, bf16[1,4096,128]{2,1,0:T(8,128)(2,1)S(1)} %copy-done.11, f32[64,1,6,128]{3,0,2,1:T(8,128)S(1)} %fusion.4), kind=kOutput, calls=%fused_computation.2 | convolution fusion | flops 807174144 | bytes 8585216 | tf_op jit(solution)/shard_map/sjcf,jfd->sjcd/dot_general | solution.py:266
  236.9 5.6 %copy.43 = bf16[64,6,4096]{2,1,0:T(8,128)(2,1)} copy(bf16[64,6,4096]{2,0,1:T(8,128)(2,1)} %convolution_convert_fusion.1) | data formatting | bytes 6291456 | tf_op jit(solution)/shard_map/convert_element_type | solution.py:268
  242.5 5.7 %all-to-all-start.2 = ((bf16[64,6,4096]{2,1,0:T(8,128)(2,1)}), bf16[64,6,4096]{2,1,0:T(8,128)(2,1)}, u32[]{:S(2)}, u32[]{:S(2)}) async-start(bf16[64,6,4096]{2,1,0:T(8,128)(2,1)} %copy.43), calls=%async_computation.2 | async-start | bytes 8388608 | tf_op jit(solution)/shard_map/all_to_all | solution.py:269
  248.6 2.7 fusion.50
  251.3 4.2 %convolution_convert_fusion.2 = bf16[256,4096]{1,0:T(8,128)(2,1)} fusion(bf16[128,4096]{1,0:T(8,128)(2,1)} %param.33, bf16[256,4096]{1,0:T(8,128)(2,1)S(1)} %copy-done.7, bf16[4096,128]{1,0:T(8,128)(2,1)} %param.32, f32[256,128]{1,0:T(8,128)S(1)} %fusion.50), kind=kOutput, calls=%fused_computation.3 | convolution fusion | flops 538116096 | bytes 6422528 | tf_op jit(solution)/shard_map/dot_general | solution.py:235
  255.8 88.7 %all-to-all-done.2 = bf16[64,6,4096]{2,1,0:T(8,128)(2,1)} async-done(((bf16[64,6,4096]{2,1,0:T(8,128)(2,1)}), bf16[64,6,4096]{2,1,0:T(8,128)(2,1)}, u32[]{:S(2)}, u32[]{:S(2)}) %all-to-all-start.2) | async-done | bytes 3145760 | tf_op jit(solution)/shard_map/all_to_all | solution.py:269
  344.5 5.7 %reshape.111 = bf16[384,4096]{1,0:T(8,128)(2,1)} reshape(bf16[64,6,4096]{2,1,0:T(8,128)(2,1)} %all-to-all-done.2) | data formatting | bytes 6291456 | tf_op jit(solution)/shard_map/reshape | solution.py:273
  350.2 6.2 %gather_fusion = bf16[256,4096]{1,0:T(8,128)(2,1)S(1)} fusion(bf16[384,4096]{1,0:T(8,128)(2,1)} %reshape.111, s32[1024]{0:T(1024)S(1)} %pad_clamp_fusion), kind=kCustom, calls=%fused_computation | custom fusion | bytes 4195328 | tf_op jit(solution)/shard_map/gather | solution.py:273
  356.4 3.0 reshape.112
  359.4 5.3 %multiply_reduce_fusion = f32[64,4096]{1,0:T(8,128)S(1)} fusion(f32[64,4,4096]{2,1,0:T(4,128)} %reshape.112, f32[64,4]{1,0:T(8,128)S(1)} %copy.44), kind=kLoop, calls=%fused_computation.5 | loop fusion | flops 1835008 | bytes 5243904 | tf_op jit(solution)/shard_map/reduce_sum | solution.py:277
  364.8 2.0 fusion.26
  (57 shorter events, 6.5 us)
Async XLA Ops:
  6.5 223.0 %copy-start = (bf16[1,128,4096]{2,1,0:T(8,128)(2,1)S(1)}, bf16[1,128,4096]{2,1,0:T(8,128)(2,1)}, u32[]{:S(2)}) copy-start(bf16[1,128,4096]{2,1,0:T(8,128)(2,1)} %param.30) | copy-start | bytes 3145732
  6.5 1.0 copy-start.1
  7.5 0.9 copy-start.2
  8.4 0.9 copy-start.3
  9.3 0.8 copy-start.4
  10.2 0.8 copy-start.5
  11.0 0.7 copy-start.6
  77.9 4.4 %copy-start.14 = (s32[64,4]{0,1:T(4,128)S(1)}, s32[64,4]{0,1:T(4,128)}, u32[]{:S(2)}) copy-start(s32[64,4]{0,1:T(4,128)} %param.26) | copy-start | bytes 3076
  77.9 31.6 %all-to-all-start = ((bf16[4,64,4096]{2,1,0:T(8,128)(2,1)}), bf16[4,64,4096]{2,1,0:T(8,128)(2,1)S(1)}, u32[]{:S(2)}, u32[]{:S(2)}) async-start(bf16[4,64,4096]{2,1,0:T(8,128)(2,1)} %bitcast.64), calls=%async_computation | async-start | bytes 4194304 | tf_op jit(solution)/shard_map/all_to_all | solution.py:226
  82.7 28.8 %copy-start.13 = (f32[4096]{0:T(1024)S(1)}, f32[4096]{0:T(1024)}, u32[]{:S(2)}) copy-start(f32[4096]{0:T(1024)} %param.25) | copy-start | bytes 49156
  109.6 1.0 copy-start.12
  110.7 0.8 copy-start.8
  111.7 8.4 %copy-start.10 = (bf16[64,4096]{1,0:T(8,128)(2,1)}, bf16[64,4096]{1,0:T(8,128)(2,1)S(1)}, u32[]{:S(2)}) copy-start(bf16[64,4096]{1,0:T(8,128)(2,1)S(1)} %fusion.24) | copy-start | bytes 1572868
  120.1 103.5 %all-to-all-start.1 = ((bf16[64,6,4096]{2,1,0:T(8,128)(2,1)}), bf16[64,6,4096]{2,1,0:T(8,128)(2,1)}, u32[]{:S(2)}, u32[]{:S(2)}) async-start(bf16[64,6,4096]{2,1,0:T(8,128)(2,1)} %reshape.106), calls=%async_computation.1 | async-start | bytes 8388608 | tf_op jit(solution)/shard_map/all_to_all | solution.py:260
  127.5 102.0 %copy-start.11 = (bf16[1,4096,128]{2,1,0:T(8,128)(2,1)S(1)}, bf16[1,4096,128]{2,1,0:T(8,128)(2,1)}, u32[]{:S(2)}) copy-start(bf16[1,4096,128]{2,1,0:T(8,128)(2,1)} %param.29) | copy-start | bytes 3145732
  127.5 121.0 %all-gather.2.cloned.1.call-start = ((), (), s32[]{:S(2)}) async-start(), calls=%async_computation.4 | async-start | bytes 2621440 | tf_op jit(solution)/shard_map/all_gather | solution.py:231
  242.5 101.9 %all-to-all-start.2 = ((bf16[64,6,4096]{2,1,0:T(8,128)(2,1)}), bf16[64,6,4096]{2,1,0:T(8,128)(2,1)}, u32[]{:S(2)}, u32[]{:S(2)}) async-start(bf16[64,6,4096]{2,1,0:T(8,128)(2,1)} %copy.43), calls=%async_computation.2 | async-start | bytes 8388608 | tf_op jit(solution)/shard_map/all_to_all | solution.py:269
  248.3 116.5 %reduce-scatter.2.cloned.1.call-start = ((), (), s32[]{:S(2)}) async-start(), calls=%async_computation.5 | async-start | bytes 2621440 | tf_op jit(solution)/shard_map/reduce_scatter | solution.py:236
  248.5 2.7 copy-start.7
  251.3 4.4 %copy-start.15 = (f32[64,4]{0,1:T(4,128)S(1)}, f32[64,4]{0,1:T(4,128)}, u32[]{:S(2)}) copy-start(f32[64,4]{0,1:T(4,128)} %param.27) | copy-start | bytes 3076
  359.4 5.4 %copy-start.9 = (bf16[64,4096]{1,0:T(8,128)(2,1)S(1)}, bf16[64,4096]{1,0:T(8,128)(2,1)}, u32[]{:S(2)}) copy-start(bf16[64,4096]{1,0:T(8,128)(2,1)} %copy-done.8) | copy-start | bytes 1572868
Sparse Core Ops, SparseCore 0:
  130.1 32.5 all-gather.1
  255.7 31.5 reduce-scatter.1

commit v2 on v1

--- a/solution.py
+++ b/solution.py
@@ -1,6 +1,3 @@
-import functools
-import math
-
 import jax
 import jax.numpy as jnp
 from jax import lax
@@ -215,66 +212,385 @@
     )(head_lambda, q_first, q_second, k_first, k_second, values)
 
 
-def cut_along(x, dim, count):
-    shape = x.shape
-    pieces = x.reshape(*shape[:dim], count, shape[dim] // count, *shape[dim + 1 :])
-    return jnp.moveaxis(pieces, dim, 0)
-
-
-def sum_at_owner(x, axis, dim):
-    count = lax.axis_size(axis)
-    pieces = lax.all_to_all(cut_along(x, dim, count), axis, 0, 0, tiled=True)
-    return jnp.sum(pieces.astype(jnp.float32), axis=0)
-
-
-def shared_part(normed, s_gate, s_up, s_down):
-    piece = lax.all_gather(normed, "tp", axis=0, tiled=True)
-    gate_part = jnp.dot(piece, s_gate, preferred_element_type=jnp.float32)
-    up_part = jnp.dot(piece, s_up, preferred_element_type=jnp.float32)
-    hidden = (jax.nn.silu(gate_part) * up_part).astype(jnp.bfloat16)
-    terms = jnp.dot(hidden, s_down, preferred_element_type=jnp.float32)
-    return lax.psum_scatter(
-        terms.astype(jnp.bfloat16), "tp", scatter_dimension=0, tiled=True
-    ).astype(jnp.float32)
-
-
-def routed_part(normed, routes, route_w, w_gate, w_up, w_down):
-    rows, topk = routes.shape
-    local_experts = w_gate.shape[0]
-    experts = local_experts * lax.axis_size("sp")
-    slots = max(2, 3 * rows * topk // (2 * experts))
-    flat_ids = routes.reshape(-1)
-    hits = (flat_ids[:, None] == jnp.arange(experts, dtype=jnp.int32)[None, :]).astype(jnp.int32)
-    slot_of = jnp.sum(jnp.cumsum(hits, axis=0) * hits, axis=1) - 1
-    target = flat_ids * slots + slot_of
-    placing = jnp.any(
-        jnp.arange(experts * slots, dtype=jnp.int32)[:, None, None]
-        == target.reshape(rows, topk)[None, :, :],
-        axis=-1,
-    ).astype(jnp.bfloat16)
-    outgoing = (
-        jnp.dot(placing, normed, preferred_element_type=jnp.float32)
-        .astype(jnp.bfloat16)
-        .reshape(experts, slots, normed.shape[1])
+D = 4096
+ROWS = 64
+TP = 4
+SLAB = 2 * NY
+CAP = 6
+GROUP = NZ * CAP
+SLOTS = SLAB * GROUP
+NC = 8
+W = D // NC
+F = 128
+MESH = pl.DeviceIdType.MESH
+DISPATCH_LAGS = (1, 2, 3, 4, 5)
+RETURN_LAGS = (1, 2, 4, 7, 9)
+
+
+def moe_kernel(
+    attn_ref, stream_ref, gain_ref, codes_ref,
+    w_out_hbm, wg_hbm, wu_hbm, wd_hbm, sg_hbm, su_hbm, sd_hbm,
+    out_ref,
+    wo, wgu, wd, sgu, sd,
+    op_all, op_in, resid_s, zbuf, cbuf, place_s, back_hi, back_lo,
+    ysend, xbuf, hid_s, hb_s, rsend, ret, part_s, rs_out, rs_in,
+    sh_all, sh_out, sh_in,
+    wo_sem, load_sem, send_sem, op_sem, z_sem, code_sem, y_sem, r_sem, rs_sem, sh_sem, shr_sem,
+):
+    me = lax.axis_index("sp")
+    tp = lax.axis_index("tp")
+    mine = me % SLAB
+    z = me // SLAB
+
+    def to_z(step):
+        return {"sp": ((z + step + NZ) % NZ) * SLAB + mine}
+
+    def to_slab(step):
+        return {"sp": z * SLAB + (mine + step) % SLAB}
+
+    def to_tp(step):
+        return {"tp": (tp + step) % TP}
+
+    def remote(src, dst, group, sem, device):
+        return pltpu.make_async_remote_copy(
+            src_ref=src, dst_ref=dst, send_sem=send_sem.at[group], recv_sem=sem,
+            device_id=device, device_id_type=MESH,
+        )
+
+    def arrived(ref, sem):
+        remote(ref, ref, 0, sem, to_z(1)).wait_recv()
+
+    def left(ref, group):
+        remote(ref, ref, group, load_sem.at[0], to_z(1)).wait_send()
+
+    def cols(k):
+        return pl.ds(pl.multiple_of(k * W, W), W)
+
+    def rows(first, count):
+        return pl.ds(pl.multiple_of(first, 16), count)
+
+    def wo_load(k):
+        return pltpu.make_async_copy(w_out_hbm.at[:, cols(k)], wo.at[:, cols(k)], wo_sem.at[k])
+
+    for k in range(NC):
+        wo_load(k).start()
+    loads = [
+        pltpu.make_async_copy(wg_hbm.at[0], wgu.at[:, 0:F], load_sem.at[0]),
+        pltpu.make_async_copy(wu_hbm.at[0], wgu.at[:, F : 2 * F], load_sem.at[1]),
+        pltpu.make_async_copy(wd_hbm.at[0], wd, load_sem.at[2]),
+        pltpu.make_async_copy(sg_hbm, sgu.at[:, 0:F], load_sem.at[3]),
+        pltpu.make_async_copy(su_hbm, sgu.at[:, F : 2 * F], load_sem.at[4]),
+        pltpu.make_async_copy(sd_hbm, sd, load_sem.at[5]),
+    ]
+    for load in loads:
+        load.start()
+
+    barrier = pltpu.get_barrier_semaphore()
+    peers = [to_z(s) for s in range(1, NZ)] + [to_slab(s) for s in range(1, SLAB)]
+    peers += [to_tp(s) for s in range(1, TP)]
+    for peer in peers:
+        pl.semaphore_signal(barrier, inc=1, device_id=peer, device_id_type=MESH)
+    cbuf[z] = codes_ref[...]
+    pl.semaphore_wait(barrier, len(peers))
+
+    for s in range(1, NZ):
+        remote(codes_ref, cbuf.at[z], 0, code_sem, to_z(s)).start()
+
+    def project(k, carry):
+        wo_load(k).wait()
+        op_all[k] = jnp.dot(
+            attn_ref[...], wo[:, cols(k)], preferred_element_type=jnp.float32
+        ).astype(jnp.bfloat16)
+        for r in range(1, TP):
+            src = op_all.at[k, rows(((tp + r) % TP) * ROWS, ROWS), :]
+            remote(src, op_in.at[k, (r - 1) * ROWS : r * ROWS, :], 1, op_sem.at[k], to_tp(r)).start()
+        return carry
+
+    lax.fori_loop(0, NC, project, 0)
+
+    arrived(cbuf.at[0 : NZ - 1], code_sem)
+    slot = lax.broadcasted_iota(jnp.int32, (SLOTS, 128), 0).astype(jnp.float32)
+    lane = lax.broadcasted_iota(jnp.int32, (SLOTS, 128), 1).astype(jnp.float32)
+    expert = jnp.floor((slot + 0.5) * (1.0 / GROUP))
+    inside = slot - expert * GROUP
+    source = jnp.floor((inside + 0.5) * (1.0 / CAP))
+    want = (z * SLAB * CAP).astype(jnp.float32) + expert * CAP + (inside - source * CAP)
+    for q in range(NZ // 2):
+        both = cbuf[2 * q] + cbuf[2 * q + 1]
+        of_me = source == (2.0 * q + jnp.floor(lane * (1.0 / ROWS)))
+        weight = jnp.zeros((SLOTS, 128), jnp.float32)
+        hit = jnp.zeros((SLOTS, 128), jnp.float32)
+        for j in range(4):
+            same = of_me & (both[j : j + 1, :] == want)
+            hit = hit + jnp.where(same, 1.0, 0.0)
+            weight = weight + jnp.where(same, both[4 + j : 5 + j, :], 0.0)
+        place_s[:, q * 128 : (q + 1) * 128] = hit.astype(jnp.bfloat16)
+        turned = weight.T
+        high = turned.astype(jnp.bfloat16)
+        back_hi[q * 128 : (q + 1) * 128, :] = high
+        back_lo[q * 128 : (q + 1) * 128, :] = (turned - high.astype(jnp.float32)).astype(jnp.bfloat16)
+
+    def residual(k, square):
+        arrived(op_in.at[k], op_sem.at[k])
+        total = op_all[k, rows(tp * ROWS, ROWS), :].astype(jnp.float32)
+        for r in range(TP - 1):
+            total = total + op_in[k, r * ROWS : (r + 1) * ROWS, :].astype(jnp.float32)
+        resid = (stream_ref[:, cols(k)].astype(jnp.float32) + total).astype(jnp.bfloat16)
+        resid_s[k] = resid
+        wide = resid.astype(jnp.float32)
+        wide = wide * wide
+        for t in range(W // 128):
+            square = square + wide[:, t * 128 : (t + 1) * 128]
+        return square
+
+    square = lax.fori_loop(0, NC, residual, jnp.zeros((ROWS, 128), jnp.float32))
+    inverse = lax.rsqrt(jnp.sum(square, axis=1, keepdims=True) * (1.0 / D) + 1e-06)
+
+    def normalize(k, carry):
+        normed = (resid_s[k].astype(jnp.float32) * inverse * gain_ref[:, cols(k)]).astype(jnp.bfloat16)
+        zbuf[k, rows(z * ROWS, ROWS), :] = normed
+        sh_all[k, 0:ROWS, :] = normed
+        return carry
+
+    lax.fori_loop(0, NC, normalize, 0)
+    for r in range(1, TP):
+        remote(
+            sh_all.at[:, 0:ROWS, :], sh_all.at[:, r * ROWS : (r + 1) * ROWS, :], 2, sh_sem, to_tp(r)
+        ).start()
+    for load in loads:
+        load.wait()
+    hid_s[...] = jnp.zeros_like(hid_s)
+
+    def pass_rows(k, owner, first, count, way):
+        ref = zbuf.at[k, rows(owner * ROWS + first, count), :]
+        remote(ref, ref, 3, z_sem.at[k, owner], to_z(way)).start()
+
+    def relay(k, step):
+        below, above = (z - step + NZ) % NZ, (z + step) % NZ
+        arrived(zbuf.at[k, rows(below * ROWS, ROWS), :], z_sem.at[k, below])
+        pass_rows(k, below, 0, ROWS if step < 3 else ROWS // 2, 1)
+        arrived(zbuf.at[k, rows(above * ROWS, ROWS), :], z_sem.at[k, above])
+        if step < 3:
+            pass_rows(k, above, 0, ROWS, -1)
+        else:
+            pass_rows(k, above, ROWS // 2, ROWS // 2, -1)
+
+    def spread(store, landing, k, sem, group):
+        for s in (2, 6, 1, 3, 5, 7, 4):
+            src = store.at[k, rows(((mine + s) % SLAB) * GROUP, GROUP), :]
+            dst = landing.at[k, rows(mine * GROUP, GROUP), :]
+            remote(src, dst, group, sem.at[k], to_slab(s)).start()
+        landing[k, rows(mine * GROUP, GROUP), :] = store[k, rows(mine * GROUP, GROUP), :]
+
+    def pack(k):
+        far = (z + 4) % NZ
+        arrived(zbuf.at[k, rows(far * ROWS, ROWS), :], z_sem.at[k, far])
+        ysend[k] = jnp.dot(
+            place_s[...], zbuf[k], preferred_element_type=jnp.float32
+        ).astype(jnp.bfloat16)
+        spread(ysend, xbuf, k, y_sem, 4)
+
+    def enter(k):
+        arrived(xbuf.at[k, 0 : SLOTS - GROUP, :], y_sem.at[k])
+        hid_s[...] += jnp.dot(xbuf[k], wgu[cols(k), :], preferred_element_type=jnp.float32)
+
+    def shared():
+        arrived(sh_all.at[:, ROWS : TP * ROWS, :], sh_sem)
+
+        def gate(k, acc):
+            return acc + jnp.dot(sh_all[k], sgu[cols(k), :], preferred_element_type=jnp.float32)
+
+        acc = lax.fori_loop(0, NC, gate, jnp.zeros((TP * ROWS, 2 * F), jnp.float32))
+        g = acc[:, 0:F]
+        hidden = (g / (1.0 + jnp.exp(-g)) * acc[:, F : 2 * F]).astype(jnp.bfloat16)
+
+        def down(k, carry):
+            sh_out[k] = jnp.dot(
+                hidden, sd[:, cols(k)], preferred_element_type=jnp.float32
+            ).astype(jnp.bfloat16)
+            for r in range(1, TP):
+                remote(
+                    sh_out.at[k, r * ROWS : (r + 1) * ROWS, :],
+                    sh_in.at[k, (r - 1) * ROWS : r * ROWS, :],
+                    5, shr_sem.at[k], to_tp(TP - r),
+                ).start()
+            return carry
+
+        lax.fori_loop(0, NC, down, 0)
+
+    def guarded(k, action):
+        @pl.when((k >= 0) & (k < NC))
+        def _():
+            action(k)
+
+    a1, a2, a3, a4, a5 = DISPATCH_LAGS
+
+    def dispatch(t, carry):
+        def own(k):
+            pass_rows(k, z, 0, ROWS, 1)
+            pass_rows(k, z, 0, ROWS, -1)
+
+        guarded(t, own)
+        guarded(t - a1, lambda k: relay(k, 1))
+        guarded(t - a2, lambda k: relay(k, 2))
+        guarded(t - a3, lambda k: relay(k, 3))
+        guarded(t - a4, pack)
+        guarded(t - a5, enter)
+
+        @pl.when(t == NC)
+        def _():
+            shared()
+
+        return carry
+
+    lax.fori_loop(0, NC + a5, dispatch, 0)
+
+    g = hid_s[:, 0:F]
+    hb_s[...] = (g / (1.0 + jnp.exp(-g)) * hid_s[:, F : 2 * F]).astype(jnp.bfloat16)
+
+    half = ROWS // 2
+
+    def leave(k):
+        rsend[k] = jnp.dot(
+            hb_s[...], wd[:, cols(k)], preferred_element_type=jnp.float32
+        ).astype(jnp.bfloat16)
+        spread(rsend, ret, k, r_sem, 6)
+
+    def hand_on(d, k, stage, first, count):
+        src = rs_out.at[d, k, stage, first : first + count, :]
+        dst = rs_in.at[d, k, stage, first : first + count, :]
+        remote(src, dst, 7, rs_sem.at[d, k, stage], to_z(1 - 2 * d)).start()
+
+    def combine(k):
+        arrived(ret.at[k, 0 : SLOTS - GROUP, :], r_sem.at[k])
+        part_s[k] = jnp.dot(
+            back_hi[...], ret[k], preferred_element_type=jnp.float32
+        ) + jnp.dot(back_lo[...], ret[k], preferred_element_type=jnp.float32)
+        owner = (z + 4) % NZ
+        for d in range(2):
+            piece = part_s[k, rows(owner * ROWS + d * half, half), :]
+            rs_out[d, k, 0, d * half : (d + 1) * half, :] = piece.astype(jnp.bfloat16)
+            hand_on(d, k, 0, d * half, half)
+
+    def add_on(k, stage):
+        for d in range(2):
+            owner = (z + (1 - 2 * d) * (4 - stage) + NZ) % NZ
+            first = d * half if stage == 1 else 0
+            count = half if stage == 1 else ROWS
+            arrived(rs_in.at[d, k, stage - 1, first : first + count, :], rs_sem.at[d, k, stage - 1])
+            piece = part_s[k, rows(owner * ROWS + first, count), :]
+            piece = piece + rs_in[d, k, stage - 1, first : first + count, :].astype(jnp.float32)
+            rs_out[d, k, stage, first : first + count, :] = piece.astype(jnp.bfloat16)
+            if stage == 1:
+                other = (1 - d) * half
+                piece = part_s[k, rows(owner * ROWS + other, half), :]
+                rs_out[d, k, stage, other : other + half, :] = piece.astype(jnp.bfloat16)
+            hand_on(d, k, stage, 0, ROWS)
+
+    def finish(k):
+        total = part_s[k, rows(z * ROWS, ROWS), :]
+        for d in range(2):
+            arrived(rs_in.at[d, k, 3], rs_sem.at[d, k, 3])
+            total = total + rs_in[d, k, 3].astype(jnp.float32)
+        arrived(sh_in.at[k], shr_sem.at[k])
+        total = total + sh_out[k, 0:ROWS, :].astype(jnp.float32)
+        for r in range(TP - 1):
+            total = total + sh_in[k, r * ROWS : (r + 1) * ROWS, :].astype(jnp.float32)
+        out_ref[:, cols(k)] = (resid_s[k].astype(jnp.float32) + total).astype(jnp.bfloat16)
+
+    b1, b2, b3, b4, b5 = RETURN_LAGS
+
+    def give_back(t, carry):
+        guarded(t, leave)
+        guarded(t - b4, lambda k: add_on(k, 3))
+        guarded(t - b3, lambda k: add_on(k, 2))
+        guarded(t - b2, lambda k: add_on(k, 1))
+        guarded(t - b1, combine)
+        guarded(t - b5, finish)
+        return carry
+
+    lax.fori_loop(0, NC + b5, give_back, 0)
+
+    left(cbuf.at[0 : NZ - 1], 0)
+    left(op_in, 1)
+    left(sh_all.at[:, ROWS : TP * ROWS, :], 2)
+    left(zbuf.at[:, 0 : 7 * ROWS, :], 3)
+    left(xbuf.at[:, 0 : SLOTS - GROUP, :], 4)
+    left(sh_in, 5)
+    left(ret.at[:, 0 : SLOTS - GROUP, :], 6)
+    left(zbuf.at[:, 0 : 7 * ROWS, :], 7)
+
+
+def moe(attn_rows, stream_in, norm_gain, codes, w_out, w_gate, w_up, w_down, s_gate, s_up, s_down):
+    vmem = pl.BlockSpec(memory_space=pltpu.VMEM)
+    hbm = pl.BlockSpec(memory_space=pl.ANY)
+    bf, f32 = jnp.bfloat16, jnp.float32
+    dma = pltpu.SemaphoreType.DMA
+    return pl.pallas_call(
+        moe_kernel,
+        out_shape=jax.ShapeDtypeStruct((ROWS, D), bf),
+        in_specs=[vmem] * 4 + [hbm] * 7,
+        out_specs=vmem,
+        scratch_shapes=[
+            pltpu.VMEM((2 * VD, D), bf),
+            pltpu.VMEM((D, 2 * F), bf),
+            pltpu.VMEM((F, D), bf),
+            pltpu.VMEM((D, 2 * F), bf),
+            pltpu.VMEM((F, D), bf),
+            pltpu.VMEM((NC, TP * ROWS, W), bf),
+            pltpu.VMEM((NC, (TP - 1) * ROWS, W), bf),
+            pltpu.VMEM((NC, ROWS, W), bf),
+            pltpu.VMEM((NC, NZ * ROWS, W), bf),
+            pltpu.VMEM((NZ, 8, 128), f32),
+            pltpu.VMEM((SLOTS, NZ * ROWS), bf),
+            pltpu.VMEM((NZ * ROWS, SLOTS), bf),
+            pltpu.VMEM((NZ * ROWS, SLOTS), bf),
+            pltpu.VMEM((NC, SLOTS, W), bf),
+            pltpu.VMEM((NC, SLOTS, W), bf),
+            pltpu.VMEM((SLOTS, 2 * F), f32),
+            pltpu.VMEM((SLOTS, F), bf),
+            pltpu.VMEM((NC, SLOTS, W), bf),
+            pltpu.VMEM((NC, SLOTS, W), bf),
+            pltpu.VMEM((NC, NZ * ROWS, W), f32),
+            pltpu.VMEM((2, NC, 4, ROWS, W), bf),
+            pltpu.VMEM((2, NC, 4, ROWS, W), bf),
+            pltpu.VMEM((NC, TP * ROWS, W), bf),
+            pltpu.VMEM((NC, TP * ROWS, W), bf),
+            pltpu.VMEM((NC, (TP - 1) * ROWS, W), bf),
+            dma((NC,)),
+            dma((6,)),
+            dma((8,)),
+            dma((NC,)),
+            dma((NC, NZ)),
+            dma,
+            dma((NC,)),
+            dma((NC,)),
+            dma((2, NC, 4)),
+            dma,
+            dma((NC,)),
+        ],
+        compiler_params=pltpu.CompilerParams(
+            collective_id=1, has_side_effects=True, vmem_limit_bytes=63 * 1024 * 1024
+        ),
+        name="experts",
+    )(attn_rows, stream_in, norm_gain.reshape(1, D), codes, w_out, w_gate, w_up, w_down, s_gate, s_up, s_down)
+
+
+def slot_codes(routes, route_w):
+    flat = routes.reshape(-1)
+    count = flat.shape[0]
+    hits = (flat[:, None] == jnp.arange(NZ * SLAB, dtype=jnp.int32)[None, :]).astype(jnp.bfloat16)
+    at = jnp.arange(count, dtype=jnp.int32)
+    earlier = (at[None, :] < at[:, None]).astype(jnp.bfloat16)
+    before = jnp.dot(earlier, hits, preferred_element_type=jnp.float32)
+    slot = jnp.sum(before * hits.astype(jnp.float32), axis=1)
+    codes = flat.astype(jnp.float32) * CAP + slot
+    table = jnp.concatenate([codes.reshape(routes.shape).T, route_w.T], axis=0)
+    blank = jnp.zeros_like(table)
+    odd = (lax.axis_index("sp") // SLAB) % 2 == 1
+    return jnp.where(
+        odd, jnp.concatenate([blank, table], axis=1), jnp.concatenate([table, blank], axis=1)
     )
-    arrived = lax.all_to_all(outgoing, "sp", split_axis=0, concat_axis=0, tiled=True)
-    sources = arrived.shape[0] // local_experts
-    grouped = arrived.reshape(sources, local_experts, arrived.shape[1], arrived.shape[2])
-    gate_part = jnp.einsum("sjcd,jdf->sjcf", grouped, w_gate, preferred_element_type=jnp.float32)
-    up_part = jnp.einsum("sjcd,jdf->sjcf", grouped, w_up, preferred_element_type=jnp.float32)
-    hidden = (jax.nn.silu(gate_part) * up_part).astype(jnp.bfloat16)
-    result = jnp.einsum(
-        "sjcf,jfd->sjcd", hidden, w_down, preferred_element_type=jnp.float32
-    ).astype(jnp.bfloat16)
-    returned = lax.all_to_all(
-        result.reshape(arrived.shape), "sp", split_axis=0, concat_axis=0, tiled=True
-    )
-    picked = (
-        returned.reshape(experts * slots, normed.shape[1])[target]
-        .reshape(rows, topk, normed.shape[1])
-        .astype(jnp.float32)
-    )
-    return jnp.sum(picked * route_w[..., None], axis=1)
 
 
 def local(
@@ -296,18 +612,11 @@
     s_up,
     s_down,
 ):
+    codes = slot_codes(routes, route_w)
     attn_rows = attention(head_lambda, q_first, q_second, k_first, k_second, values)
-    attn = sum_at_owner(
-        jnp.dot(attn_rows, w_out, preferred_element_type=jnp.float32).astype(jnp.bfloat16), "tp", 0
+    return moe(
+        attn_rows, stream_in, norm_gain, codes, w_out, w_gate, w_up, w_down, s_gate, s_up, s_down
     )
-    resid = (stream_in.astype(jnp.float32) + attn).astype(jnp.bfloat16)
-    stream = lax.optimization_barrier(resid).astype(jnp.float32)
-    normed = (
-        stream * lax.rsqrt(jnp.mean(stream * stream, axis=-1, keepdims=True) + 1e-06) * norm_gain
-    ).astype(jnp.bfloat16)
-    routed = routed_part(normed, routes, route_w, w_gate, w_up, w_down)
-    shared = shared_part(normed, s_gate, s_up, s_down)
-    return (stream + routed + shared).astype(jnp.bfloat16)
 
 
 def solution(mesh):

time: 375 us -> 224 us (0.60)
  waiting for transfers between devices: 210 us -> 0 us
  Pallas kernels: 61.5 us -> 212 us
  matrix products: 27.7 us -> 0.21 us
  local copies, waits for them, and re-layouts: 33.6 us -> 8.66 us
  starting transfers between devices: 18 us -> 0 us
  between operations: 13.6 us -> 0.05 us
  other arithmetic: 9.07 us -> 2.05 us
    all_to_all x3 -> x0, waiting for transfers between devices: 210 us -> none  [the longest x1 95.3 us: routed_part(): lax.all_to_all(outgoing, 'sp', split_axis=0, concat_axis=0, tiled=True)]
    pallas_call x0 -> x1, Pallas kernels: none -> 150 us  [moe(): pl.pallas_call(moe_kernel, out_shape=jax.ShapeDtypeStruct((ROWS, D), bf),...]
    dot_general x6 -> x1, matrix products: 27.7 us -> 0.21 us  [slot_codes(): before = jnp.dot(earlier, hits, preferred_element_type=jnp.float32)]
    all_to_all x3 -> x0, starting transfers between devices: 17.5 us -> none  [the longest x1 7.41 us: routed_part(): lax.all_to_all(outgoing, 'sp', split_axis=0, concat_axis=0, tiled=True)]
    reshape x2 -> x0, local copies, waits for them, and re-layouts: 11.4 us -> none  [the longest x1 5.74 us: routed_part(): returned.reshape(experts * slots, normed.shape[1])[target]]
    convert_element_type x2 -> x0, local copies, waits for them, and re-layouts: 8.63 us -> none  [the longest x1 5.62 us: routed_part(): result = jnp.einsum('sjcf,jfd->sjcd', hidden, w_down, preferred_element_t...]
    gather x1 -> x0, local copies, waits for them, and re-layouts: 6.18 us -> none  [routed_part(): returned.reshape(experts * slots, normed.shape[1])[target]]
    reduce_sum x4 -> x0, other arithmetic: 5.98 us -> none  [the longest x1 5.34 us: routed_part(): return jnp.sum(picked * route_w[..., None], axis=1)]
  transfers between devices with their start and end apart: 5 -> 0, of which waited for: 3 -> 0; matrix products, arithmetic and copies ran while one was open for 13% -> 0% of each run, Pallas kernels for 0% -> 0%
where the time goes in v2:
time: 224 us; the launch traced here: 223 us
  Pallas kernels  212 us (95%)
  local copies, waits for them, and re-layouts  8.66 us (4%)
    pallas_call x1, Pallas kernels, moe(): pl.pallas_call(moe_kernel, out_shape=jax.ShapeDtypeStruct((ROWS, D), bf),...  150 us
    pallas_call x1, Pallas kernels, attention(): pl.pallas_call(attn_kernel, out_shape=jax.ShapeDtypeStruct((BLK, 2 * VD),...  61.5 us
    unnamed x16, local copies, waits for them, and re-layouts  8.38 us

profile of v2, /device:TPU:8, one launch (start us, length us, event | category | flops | bytes accessed | tf_op | source)
XLA Modules:
  0.0 222.6 jit_solution(14238444801901263953)
XLA Ops:
  0.0 0.8 copy.18
  0.8 0.1 eq.21
  0.9 0.2 fusion
  1.1 0.1 reduce_sum.12
  1.2 0.1 copy.19
  1.3 0.7 add_bitcast_fusion
  2.0 0.7 pad_maximum_fusion
  2.7 0.7 pad_select_fusion.codes_ref
  3.3 0.0 copy-start.1
  3.3 0.9 copy-done.1
  4.2 0.0 copy-start.2
  4.2 0.9 copy-done.2
  5.1 0.0 copy-start.3
  5.1 0.9 copy-done.3
  6.0 0.0 copy-start.4
  6.0 0.8 copy-done.4
  6.9 0.0 copy-start.5
  6.9 0.8 copy-done.5
  7.7 0.7 copy-done.6
  8.4 61.5 %attend.1.attn_ref = bf16[256,512]{1,0:T(8,128)(2,1)S(1)} custom-call(f32[2]{0:T(128)S(1)} %copy-done.6, bf16[256,256]{1,0:T(8,128)(2,1)S(1)} %copy-done.1, bf16[256,256]{1,0:T(8,128)(2,1)S(1)} %copy-done.2, bf16[256,128]{1,0:T(8,128)(2,1)S(1)} %copy-done.4, bf16[256,128]{1,0:T(8,128)(2,1)S(1)} %copy-done.5, bf16[256,256]{1,0:T(8,128)(2,1)S(1)} %copy-done.3), custom_call_target="tpu_custom_call" | custom-call | tf_op jit(solution)/shard_map/attend/pallas_call | solution.py:192
  69.9 0.0 copy-start
  69.9 0.7 copy-done
  70.6 150.1 %experts.1 = bf16[64,4096]{1,0:T(8,128)(2,1)} custom-call(bf16[256,512]{1,0:T(8,128)(2,1)} %copy-done, bf16[64,4096]{1,0:T(8,128)(2,1)} %stream_ref.1, f32[1,4096]{1,0:T(1,128)} %bitcast.4, f32[8,128]{1,0:T(8,128)} %pad_select_fusion.codes_ref, bf16[512,4096]{1,0:T(8,128)(2,1)} %w_out_hbm.1, bf16[1,4096,128]{2,1,0:T(8,128)(2,1)} %wg_hbm.1, ...), custom_call_target="tpu_custom_call" | custom-call | tf_op jit(solution)/shard_map/experts/pallas_call | solution.py:529
  220.7 1.9 copy.21
  (1 shorter events, 0.0 us)
Async XLA Ops:
  3.3 0.9 copy-start.1
  4.2 0.9 copy-start.2
  5.1 0.9 copy-start.3
  6.0 0.8 copy-start.4
  6.9 0.8 copy-start.5
  7.7 0.7 copy-start.6
  69.9 0.7 copy-start

commit v3 on v2

--- a/solution.py
+++ b/solution.py
@@ -53,7 +53,7 @@
 
 
 def attn_kernel(
-    lam_ref, q1_ref, q2_ref, k1_hbm, k2_hbm, v_hbm, out_ref,
+    lam_ref, q1_hbm, q2_hbm, k1_hbm, k2_hbm, v_hbm, out_ref,
     kv, q_s, m_s, l_s, acc_s, load_sem, send_sem, recv_sem, pair_sem,
 ):
     me = lax.axis_index("sp")
@@ -78,14 +78,22 @@
         loads.append(pltpu.make_async_copy(src, kv.at[pl.ds(own, BLK), lo:hi], load_sem.at[k]))
         loads[-1].start()
 
+    for k, ref in enumerate((q1_hbm, q2_hbm)):
+        for h in range(2):
+            loads.append(
+                pltpu.make_async_copy(
+                    ref.at[:, h * HEAD : (h + 1) * HEAD],
+                    q_s.at[k, h * BLK : (h + 1) * BLK, :],
+                    load_sem.at[3 + 2 * k + h],
+                )
+            )
+            loads[-1].start()
+
     barrier = pltpu.get_barrier_semaphore()
     for link in links:
         pl.semaphore_signal(barrier, inc=1, device_id=peers[link], device_id_type=pl.DeviceIdType.MESH)
 
     scale = HEAD ** (-0.5) * LOG2E
-    for k, ref in enumerate((q1_ref, q2_ref)):
-        for h in range(2):
-            q_s[k, h * BLK : (h + 1) * BLK, :] = ref[:, h * HEAD : (h + 1) * HEAD]
     m_s[...] = jnp.full_like(m_s, FLOOR)
     l_s[...] = jnp.zeros_like(l_s)
     acc_s[...] = jnp.zeros_like(acc_s)
@@ -192,7 +200,7 @@
     return pl.pallas_call(
         attn_kernel,
         out_shape=jax.ShapeDtypeStruct((BLK, 2 * VD), jnp.bfloat16),
-        in_specs=[pl.BlockSpec(memory_space=pltpu.SMEM), vmem, vmem, hbm, hbm, hbm],
+        in_specs=[pl.BlockSpec(memory_space=pltpu.SMEM)] + [hbm] * 5,
         out_specs=vmem,
         scratch_shapes=[
             pltpu.VMEM((NCHIP * PAIR, KVW), jnp.bfloat16),
@@ -200,13 +208,13 @@
             pltpu.VMEM((2, 2 * BLK, 128), jnp.float32),
             pltpu.VMEM((2, 2 * BLK, 128), jnp.float32),
             pltpu.VMEM((2, 2 * BLK, VD), jnp.float32),
-            pltpu.SemaphoreType.DMA((3,)),
+            pltpu.SemaphoreType.DMA((7,)),
             pltpu.SemaphoreType.DMA((5,)),
             pltpu.SemaphoreType.DMA((NCHIP,)),
             pltpu.SemaphoreType.DMA((NCHIP,)),
         ],
         compiler_params=pltpu.CompilerParams(
-            collective_id=0, has_side_effects=True, vmem_limit_bytes=48 * 1024 * 1024
+            collective_id=0, has_side_effects=True, vmem_limit_bytes=63 * 1024 * 1024
         ),
         name="attend",
     )(head_lambda, q_first, q_second, k_first, k_second, values)
@@ -215,32 +223,39 @@
 D = 4096
 ROWS = 64
 TP = 4
+TOPK = 4
 SLAB = 2 * NY
 CAP = 6
 GROUP = NZ * CAP
 SLOTS = SLAB * GROUP
-NC = 8
+NC = 16
 W = D // NC
 F = 128
 MESH = pl.DeviceIdType.MESH
-DISPATCH_LAGS = (1, 2, 3, 4, 5)
-RETURN_LAGS = (1, 2, 4, 7, 9)
+SUM_LAG, RESID_LAG = 3, 5
+HOP_LAGS = tuple(RESID_LAG + n for n in (3, 4, 5))
+PACK_LAG, ENTER_LAG = RESID_LAG + 6, RESID_LAG + 9
+SHARE_LAG = RESID_LAG + 4
+RETURN_LAGS = (2, 4, 6, 9, 11)
 
 
 def moe_kernel(
-    attn_ref, stream_ref, gain_ref, codes_ref,
+    attn_hbm, stream_hbm, gain_hbm, routes_ref, route_w_ref,
     w_out_hbm, wg_hbm, wu_hbm, wd_hbm, sg_hbm, su_hbm, sd_hbm,
     out_ref,
-    wo, wgu, wd, sgu, sd,
-    op_all, op_in, resid_s, zbuf, cbuf, place_s, back_hi, back_lo,
+    attn_s, stream_s, gain_s, wo, wgu, wd, sgu, sd,
+    op_all, op_out, op_in, resid_s, square_s, zbuf, cbuf, place_s, back_hi, back_lo,
+    turn_s, inv_own, inv_z, inv_send, inv_slot, inv_sh,
     ysend, xbuf, hid_s, hb_s, rsend, ret, part_s, rs_out, rs_in,
-    sh_all, sh_out, sh_in,
-    wo_sem, load_sem, send_sem, op_sem, z_sem, code_sem, y_sem, r_sem, rs_sem, sh_sem, shr_sem,
+    sh_all, sh_out, sh_pass, sh_in,
+    wo_sem, load_sem, send_sem, op_sem, z_sem, code_sem, y_sem, r_sem, rs_sem,
+    sh_sem, shr_sem, inv_z_sem, inv_slot_sem, inv_sh_sem,
 ):
     me = lax.axis_index("sp")
     tp = lax.axis_index("tp")
     mine = me % SLAB
     z = me // SLAB
+    half = ROWS // 2
 
     def to_z(step):
         return {"sp": ((z + step + NZ) % NZ) * SLAB + mine}
@@ -249,7 +264,7 @@
         return {"sp": z * SLAB + (mine + step) % SLAB}
 
     def to_tp(step):
-        return {"tp": (tp + step) % TP}
+        return {"tp": (tp + step + TP) % TP}
 
     def remote(src, dst, group, sem, device):
         return pltpu.make_async_remote_copy(
@@ -272,6 +287,13 @@
     def wo_load(k):
         return pltpu.make_async_copy(w_out_hbm.at[:, cols(k)], wo.at[:, cols(k)], wo_sem.at[k])
 
+    early = [
+        pltpu.make_async_copy(attn_hbm, attn_s, load_sem.at[6]),
+        pltpu.make_async_copy(stream_hbm, stream_s, load_sem.at[7]),
+        pltpu.make_async_copy(gain_hbm, gain_s, load_sem.at[8]),
+    ]
+    for load in early:
+        load.start()
     for k in range(NC):
         wo_load(k).start()
     loads = [
@@ -290,90 +312,169 @@
     peers += [to_tp(s) for s in range(1, TP)]
     for peer in peers:
         pl.semaphore_signal(barrier, inc=1, device_id=peer, device_id_type=MESH)
-    cbuf[z] = codes_ref[...]
+
+    names = lax.broadcasted_iota(jnp.int32, (NZ * SLAB, ROWS), 0)
+    hits = jnp.zeros((NZ * SLAB, ROWS), jnp.float32)
+    for j in range(TOPK):
+        hits = hits + jnp.where(routes_ref[j : j + 1, :] == names, 1.0, 0.0)
+    upper = (
+        lax.broadcasted_iota(jnp.int32, (ROWS, ROWS), 0)
+        < lax.broadcasted_iota(jnp.int32, (ROWS, ROWS), 1)
+    )
+    before = jnp.dot(
+        hits.astype(jnp.bfloat16),
+        jnp.where(upper, 1.0, 0.0).astype(jnp.bfloat16),
+        preferred_element_type=jnp.float32,
+    )
+    table = []
+    for j in range(TOPK):
+        chosen = routes_ref[j : j + 1, :]
+        taken = jnp.sum(jnp.where(chosen == names, before, 0.0), axis=0, keepdims=True)
+        table.append(chosen.astype(jnp.float32) * CAP + taken)
+    for j in range(TOPK):
+        table.append(route_w_ref[j : j + 1, :])
+    table = jnp.concatenate(table, axis=0)
+    odd = (z % 2).astype(jnp.float32)
+    cbuf[z] = jnp.concatenate([table * (1.0 - odd), table * odd], axis=1)
+    turn_s[...] = jnp.zeros_like(turn_s)
+    square_s[...] = jnp.zeros_like(square_s)
+    hid_s[...] = jnp.zeros_like(hid_s)
+
     pl.semaphore_wait(barrier, len(peers))
-
     for s in range(1, NZ):
-        remote(codes_ref, cbuf.at[z], 0, code_sem, to_z(s)).start()
-
-    def project(k, carry):
+        remote(cbuf.at[z], cbuf.at[z], 0, code_sem, to_z(s)).start()
+    for load in early:
+        load.wait()
+
+    def ring_out(d, stage, first, count, k, src, group, landing, sem):
+        dst = landing.at[d, k, stage, first : first + count, :]
+        remote(src, dst, group, sem.at[d, k, stage], to_tp(1 - 2 * d)).start()
+
+    def ring_first(k, table_ref, landing, group, sem):
+        for d in range(2):
+            src = table_ref.at[k, rows(((tp + 2) % TP) * ROWS + d * half, half), :]
+            ring_out(d, 0, d * half, half, k, src, group, landing, sem)
+
+    def ring_second(k, table_ref, passing, landing, group, sem):
+        for d in range(2):
+            first, other = d * half, (1 - d) * half
+            owner = (tp + 1 - 2 * d + TP) % TP
+            arrived(landing.at[d, k, 0, first : first + half, :], sem.at[d, k, 0])
+            piece = table_ref[k, rows(owner * ROWS + first, half), :].astype(jnp.float32)
+            piece = piece + landing[d, k, 0, first : first + half, :].astype(jnp.float32)
+            passing[d, k, first : first + half, :] = piece.astype(jnp.bfloat16)
+            passing[d, k, other : other + half, :] = table_ref[k, rows(owner * ROWS + other, half), :]
+            ring_out(d, 1, 0, ROWS, k, passing.at[d, k], group, landing, sem)
+
+    def ring_total(k, table_ref, landing, sem):
+        total = table_ref[k, rows(tp * ROWS, ROWS), :].astype(jnp.float32)
+        for d in range(2):
+            arrived(landing.at[d, k, 1], sem.at[d, k, 1])
+            total = total + landing[d, k, 1].astype(jnp.float32)
+        return total
+
+    def project(k):
         wo_load(k).wait()
         op_all[k] = jnp.dot(
-            attn_ref[...], wo[:, cols(k)], preferred_element_type=jnp.float32
+            attn_s[...], wo[:, cols(k)], preferred_element_type=jnp.float32
         ).astype(jnp.bfloat16)
-        for r in range(1, TP):
-            src = op_all.at[k, rows(((tp + r) % TP) * ROWS, ROWS), :]
-            remote(src, op_in.at[k, (r - 1) * ROWS : r * ROWS, :], 1, op_sem.at[k], to_tp(r)).start()
-        return carry
-
-    lax.fori_loop(0, NC, project, 0)
-
-    arrived(cbuf.at[0 : NZ - 1], code_sem)
-    slot = lax.broadcasted_iota(jnp.int32, (SLOTS, 128), 0).astype(jnp.float32)
-    lane = lax.broadcasted_iota(jnp.int32, (SLOTS, 128), 1).astype(jnp.float32)
-    expert = jnp.floor((slot + 0.5) * (1.0 / GROUP))
-    inside = slot - expert * GROUP
-    source = jnp.floor((inside + 0.5) * (1.0 / CAP))
-    want = (z * SLAB * CAP).astype(jnp.float32) + expert * CAP + (inside - source * CAP)
-    for q in range(NZ // 2):
-        both = cbuf[2 * q] + cbuf[2 * q + 1]
-        of_me = source == (2.0 * q + jnp.floor(lane * (1.0 / ROWS)))
-        weight = jnp.zeros((SLOTS, 128), jnp.float32)
-        hit = jnp.zeros((SLOTS, 128), jnp.float32)
-        for j in range(4):
-            same = of_me & (both[j : j + 1, :] == want)
-            hit = hit + jnp.where(same, 1.0, 0.0)
-            weight = weight + jnp.where(same, both[4 + j : 5 + j, :], 0.0)
-        place_s[:, q * 128 : (q + 1) * 128] = hit.astype(jnp.bfloat16)
-        turned = weight.T
-        high = turned.astype(jnp.bfloat16)
-        back_hi[q * 128 : (q + 1) * 128, :] = high
-        back_lo[q * 128 : (q + 1) * 128, :] = (turned - high.astype(jnp.float32)).astype(jnp.bfloat16)
-
-    def residual(k, square):
-        arrived(op_in.at[k], op_sem.at[k])
-        total = op_all[k, rows(tp * ROWS, ROWS), :].astype(jnp.float32)
-        for r in range(TP - 1):
-            total = total + op_in[k, r * ROWS : (r + 1) * ROWS, :].astype(jnp.float32)
-        resid = (stream_ref[:, cols(k)].astype(jnp.float32) + total).astype(jnp.bfloat16)
-        resid_s[k] = resid
-        wide = resid.astype(jnp.float32)
-        wide = wide * wide
-        for t in range(W // 128):
-            square = square + wide[:, t * 128 : (t + 1) * 128]
-        return square
-
-    square = lax.fori_loop(0, NC, residual, jnp.zeros((ROWS, 128), jnp.float32))
-    inverse = lax.rsqrt(jnp.sum(square, axis=1, keepdims=True) * (1.0 / D) + 1e-06)
-
-    def normalize(k, carry):
-        normed = (resid_s[k].astype(jnp.float32) * inverse * gain_ref[:, cols(k)]).astype(jnp.bfloat16)
-        zbuf[k, rows(z * ROWS, ROWS), :] = normed
-        sh_all[k, 0:ROWS, :] = normed
-        return carry
-
-    lax.fori_loop(0, NC, normalize, 0)
-    for r in range(1, TP):
-        remote(
-            sh_all.at[:, 0:ROWS, :], sh_all.at[:, r * ROWS : (r + 1) * ROWS, :], 2, sh_sem, to_tp(r)
-        ).start()
-    for load in loads:
-        load.wait()
-    hid_s[...] = jnp.zeros_like(hid_s)
+        ring_first(k, op_all, op_in, 1, op_sem)
 
     def pass_rows(k, owner, first, count, way):
         ref = zbuf.at[k, rows(owner * ROWS + first, count), :]
         remote(ref, ref, 3, z_sem.at[k, owner], to_z(way)).start()
 
+    def share_rows(k, owner, first, count, way):
+        ref = sh_all.at[k, rows(owner * ROWS + first, count), :]
+        remote(ref, ref, 2, sh_sem.at[k, owner], to_tp(way)).start()
+
+    def residual(k):
+        total = ring_total(k, op_all, op_in, op_sem)
+        resid = (stream_s[:, cols(k)].astype(jnp.float32) + total).astype(jnp.bfloat16)
+        resid_s[k] = resid
+        wide = resid.astype(jnp.float32)
+        gain = jnp.concatenate(
+            [gain_s[pl.ds(k * (W // 128) + t, 1), :] for t in range(W // 128)], axis=1
+        )
+        scaled = (wide * gain).astype(jnp.bfloat16)
+        zbuf[k, rows(z * ROWS, ROWS), :] = scaled
+        sh_all[k, rows(tp * ROWS, ROWS), :] = scaled
+        for way in (1, -1):
+            pass_rows(k, z, 0, ROWS, way)
+            share_rows(k, tp, 0, ROWS, way)
+        wide = wide * wide
+        square = square_s[...]
+        for t in range(W // 128):
+            square = square + wide[:, t * 128 : (t + 1) * 128]
+        square_s[...] = square
+
+    def send_inverse():
+        mean = jnp.sum(square_s[...], axis=1, keepdims=True) * (1.0 / D)
+        inverse = jnp.broadcast_to(lax.rsqrt(mean + 1e-06), (ROWS, 128))
+        inv_sh[rows(tp * ROWS, ROWS), :] = inverse
+        turn_s[rows((z % 2) * ROWS, ROWS), :] = inverse
+        inv_own[...] = turn_s[...].T[0:8, :]
+        inv_z[z] = inv_own[...]
+        for s in range(1, NZ):
+            remote(inv_own, inv_z.at[z], 8, inv_z_sem, to_z(s)).start()
+        own = inv_sh.at[rows(tp * ROWS, ROWS), :]
+        for r in range(1, TP):
+            remote(own, own, 9, inv_sh_sem, to_tp(r)).start()
+
+    def spread_inverse():
+        arrived(inv_z.at[0 : NZ - 1], inv_z_sem)
+        total = jnp.zeros((SLOTS, 128), jnp.float32)
+        for q in range(NZ // 2):
+            both = inv_z[2 * q] + inv_z[2 * q + 1]
+            total = total + place_s[:, q * 128 : (q + 1) * 128].astype(jnp.float32) * both[0:1, :]
+        inv_send[...] = jnp.broadcast_to(jnp.sum(total, axis=1, keepdims=True), (SLOTS, 128))
+        land = inv_slot.at[rows(mine * GROUP, GROUP), :]
+        for s in range(1, SLAB):
+            src = inv_send.at[rows(((mine + s) % SLAB) * GROUP, GROUP), :]
+            remote(src, land, 10, inv_slot_sem, to_slab(s)).start()
+        inv_slot[rows(mine * GROUP, GROUP), :] = inv_send[rows(mine * GROUP, GROUP), :]
+
+    def places():
+        arrived(cbuf.at[0 : NZ - 1], code_sem)
+        slot = lax.broadcasted_iota(jnp.int32, (SLOTS, 128), 0).astype(jnp.float32)
+        lane = lax.broadcasted_iota(jnp.int32, (SLOTS, 128), 1).astype(jnp.float32)
+        expert = jnp.floor((slot + 0.5) * (1.0 / GROUP))
+        inside = slot - expert * GROUP
+        source = jnp.floor((inside + 0.5) * (1.0 / CAP))
+        want = (z * SLAB * CAP).astype(jnp.float32) + expert * CAP + (inside - source * CAP)
+        for q in range(NZ // 2):
+            both = cbuf[2 * q] + cbuf[2 * q + 1]
+            of_me = source == (2.0 * q + jnp.floor(lane * (1.0 / ROWS)))
+            weight = jnp.zeros((SLOTS, 128), jnp.float32)
+            hit = jnp.zeros((SLOTS, 128), jnp.float32)
+            for j in range(TOPK):
+                same = of_me & (both[j : j + 1, :] == want)
+                hit = hit + jnp.where(same, 1.0, 0.0)
+                weight = weight + jnp.where(same, both[TOPK + j : TOPK + j + 1, :], 0.0)
+            place_s[:, q * 128 : (q + 1) * 128] = hit.astype(jnp.bfloat16)
+            turned = weight.T
+            high = turned.astype(jnp.bfloat16)
+            back_hi[q * 128 : (q + 1) * 128, :] = high
+            back_lo[q * 128 : (q + 1) * 128, :] = (turned - high.astype(jnp.float32)).astype(
+                jnp.bfloat16
+            )
+
     def relay(k, step):
         below, above = (z - step + NZ) % NZ, (z + step) % NZ
         arrived(zbuf.at[k, rows(below * ROWS, ROWS), :], z_sem.at[k, below])
-        pass_rows(k, below, 0, ROWS if step < 3 else ROWS // 2, 1)
+        pass_rows(k, below, 0, ROWS if step < 3 else half, 1)
         arrived(zbuf.at[k, rows(above * ROWS, ROWS), :], z_sem.at[k, above])
         if step < 3:
             pass_rows(k, above, 0, ROWS, -1)
         else:
-            pass_rows(k, above, ROWS // 2, ROWS // 2, -1)
+            pass_rows(k, above, half, half, -1)
+
+    def share(k):
+        below, above = (tp + TP - 1) % TP, (tp + 1) % TP
+        arrived(sh_all.at[k, rows(below * ROWS, ROWS), :], sh_sem.at[k, below])
+        share_rows(k, below, 0, half, 1)
+        arrived(sh_all.at[k, rows(above * ROWS, ROWS), :], sh_sem.at[k, above])
+        share_rows(k, above, half, half, -1)
 
     def spread(store, landing, k, sem, group):
         for s in (2, 6, 1, 3, 5, 7, 4):
@@ -394,26 +495,25 @@
         arrived(xbuf.at[k, 0 : SLOTS - GROUP, :], y_sem.at[k])
         hid_s[...] += jnp.dot(xbuf[k], wgu[cols(k), :], preferred_element_type=jnp.float32)
 
+    def gated(sums, inverse):
+        g = sums[:, 0:F] * inverse
+        return (g / (1.0 + jnp.exp(-g)) * (sums[:, F : 2 * F] * inverse)).astype(jnp.bfloat16)
+
     def shared():
-        arrived(sh_all.at[:, ROWS : TP * ROWS, :], sh_sem)
-
         def gate(k, acc):
+            far = (tp + 2) % TP
+            arrived(sh_all.at[k, rows(far * ROWS, ROWS), :], sh_sem.at[k, far])
             return acc + jnp.dot(sh_all[k], sgu[cols(k), :], preferred_element_type=jnp.float32)
 
         acc = lax.fori_loop(0, NC, gate, jnp.zeros((TP * ROWS, 2 * F), jnp.float32))
-        g = acc[:, 0:F]
-        hidden = (g / (1.0 + jnp.exp(-g)) * acc[:, F : 2 * F]).astype(jnp.bfloat16)
+        arrived(inv_sh.at[0 : (TP - 1) * ROWS, :], inv_sh_sem)
+        hidden = gated(acc, inv_sh[...])
 
         def down(k, carry):
             sh_out[k] = jnp.dot(
                 hidden, sd[:, cols(k)], preferred_element_type=jnp.float32
             ).astype(jnp.bfloat16)
-            for r in range(1, TP):
-                remote(
-                    sh_out.at[k, r * ROWS : (r + 1) * ROWS, :],
-                    sh_in.at[k, (r - 1) * ROWS : r * ROWS, :],
-                    5, shr_sem.at[k], to_tp(TP - r),
-                ).start()
+            ring_first(k, sh_out, sh_in, 5, shr_sem)
             return carry
 
         lax.fori_loop(0, NC, down, 0)
@@ -423,32 +523,42 @@
         def _():
             action(k)
 
-    a1, a2, a3, a4, a5 = DISPATCH_LAGS
-
-    def dispatch(t, carry):
-        def own(k):
-            pass_rows(k, z, 0, ROWS, 1)
-            pass_rows(k, z, 0, ROWS, -1)
-
-        guarded(t, own)
-        guarded(t - a1, lambda k: relay(k, 1))
-        guarded(t - a2, lambda k: relay(k, 2))
-        guarded(t - a3, lambda k: relay(k, 3))
-        guarded(t - a4, pack)
-        guarded(t - a5, enter)
-
-        @pl.when(t == NC)
+    def way_out(t, carry):
+        guarded(t, project)
+
+        @pl.when(t == 1)
+        def _():
+            places()
+            for load in loads:
+                load.wait()
+
+        guarded(t - SUM_LAG, lambda k: ring_second(k, op_all, op_out, op_in, 1, op_sem))
+        for step in (1, 2, 3):
+            guarded(t - HOP_LAGS[step - 1], lambda k, step=step: relay(k, step))
+        guarded(t - RESID_LAG, residual)
+
+        @pl.when(t == NC - 1 + RESID_LAG)
+        def _():
+            send_inverse()
+
+        guarded(t - SHARE_LAG, share)
+        guarded(t - PACK_LAG, pack)
+        guarded(t - ENTER_LAG, enter)
+
+        @pl.when(t == NC + 1 + RESID_LAG)
+        def _():
+            spread_inverse()
+
+        @pl.when(t == NC + 2 + SHARE_LAG)
         def _():
             shared()
 
         return carry
 
-    lax.fori_loop(0, NC + a5, dispatch, 0)
-
-    g = hid_s[:, 0:F]
-    hb_s[...] = (g / (1.0 + jnp.exp(-g)) * hid_s[:, F : 2 * F]).astype(jnp.bfloat16)
-
-    half = ROWS // 2
+    lax.fori_loop(0, NC + ENTER_LAG, way_out, 0)
+
+    arrived(inv_slot.at[0 : SLOTS - GROUP, :], inv_slot_sem)
+    hb_s[...] = gated(hid_s[...], inv_slot[...])
 
     def leave(k):
         rsend[k] = jnp.dot(
@@ -492,10 +602,7 @@
         for d in range(2):
             arrived(rs_in.at[d, k, 3], rs_sem.at[d, k, 3])
             total = total + rs_in[d, k, 3].astype(jnp.float32)
-        arrived(sh_in.at[k], shr_sem.at[k])
-        total = total + sh_out[k, 0:ROWS, :].astype(jnp.float32)
-        for r in range(TP - 1):
-            total = total + sh_in[k, r * ROWS : (r + 1) * ROWS, :].astype(jnp.float32)
+        total = total + ring_total(k, sh_out, sh_in, shr_sem)
         out_ref[:, cols(k)] = (resid_s[k].astype(jnp.float32) + total).astype(jnp.bfloat16)
 
     b1, b2, b3, b4, b5 = RETURN_LAGS
@@ -506,22 +613,28 @@
         guarded(t - b3, lambda k: add_on(k, 2))
         guarded(t - b2, lambda k: add_on(k, 1))
         guarded(t - b1, combine)
+        guarded(t - b1, lambda k: ring_second(k, sh_out, sh_pass, sh_in, 5, shr_sem))
         guarded(t - b5, finish)
         return carry
 
     lax.fori_loop(0, NC + b5, give_back, 0)
 
     left(cbuf.at[0 : NZ - 1], 0)
-    left(op_in, 1)
-    left(sh_all.at[:, ROWS : TP * ROWS, :], 2)
+    left(sh_all.at[:, 0 : 3 * ROWS, :], 1)
+    left(sh_all.at[:, 0 : 3 * ROWS, :], 2)
     left(zbuf.at[:, 0 : 7 * ROWS, :], 3)
     left(xbuf.at[:, 0 : SLOTS - GROUP, :], 4)
-    left(sh_in, 5)
+    left(sh_all.at[:, 0 : 3 * ROWS, :], 5)
     left(ret.at[:, 0 : SLOTS - GROUP, :], 6)
     left(zbuf.at[:, 0 : 7 * ROWS, :], 7)
-
-
-def moe(attn_rows, stream_in, norm_gain, codes, w_out, w_gate, w_up, w_down, s_gate, s_up, s_down):
+    left(inv_z.at[0 : NZ - 1], 8)
+    left(inv_sh.at[0 : (TP - 1) * ROWS, :], 9)
+    left(inv_slot.at[0 : SLOTS - GROUP, :], 10)
+
+
+def moe(
+    attn_rows, stream_in, norm_gain, routes, route_w, w_out, w_gate, w_up, w_down, s_gate, s_up, s_down
+):
     vmem = pl.BlockSpec(memory_space=pltpu.VMEM)
     hbm = pl.BlockSpec(memory_space=pl.ANY)
     bf, f32 = jnp.bfloat16, jnp.float32
@@ -529,22 +642,33 @@
     return pl.pallas_call(
         moe_kernel,
         out_shape=jax.ShapeDtypeStruct((ROWS, D), bf),
-        in_specs=[vmem] * 4 + [hbm] * 7,
+        in_specs=[hbm] * 3 + [vmem] * 2 + [hbm] * 7,
         out_specs=vmem,
         scratch_shapes=[
+            pltpu.VMEM((TP * ROWS, 2 * VD), bf),
+            pltpu.VMEM((ROWS, D), bf),
+            pltpu.VMEM((D // 128, 128), f32),
             pltpu.VMEM((2 * VD, D), bf),
             pltpu.VMEM((D, 2 * F), bf),
             pltpu.VMEM((F, D), bf),
             pltpu.VMEM((D, 2 * F), bf),
             pltpu.VMEM((F, D), bf),
             pltpu.VMEM((NC, TP * ROWS, W), bf),
-            pltpu.VMEM((NC, (TP - 1) * ROWS, W), bf),
+            pltpu.VMEM((2, NC, ROWS, W), bf),
+            pltpu.VMEM((2, NC, 2, ROWS, W), bf),
             pltpu.VMEM((NC, ROWS, W), bf),
+            pltpu.VMEM((ROWS, 128), f32),
             pltpu.VMEM((NC, NZ * ROWS, W), bf),
             pltpu.VMEM((NZ, 8, 128), f32),
             pltpu.VMEM((SLOTS, NZ * ROWS), bf),
             pltpu.VMEM((NZ * ROWS, SLOTS), bf),
             pltpu.VMEM((NZ * ROWS, SLOTS), bf),
+            pltpu.VMEM((2 * ROWS, 128), f32),
+            pltpu.VMEM((8, 128), f32),
+            pltpu.VMEM((NZ, 8, 128), f32),
+            pltpu.VMEM((SLOTS, 128), f32),
+            pltpu.VMEM((SLOTS, 128), f32),
+            pltpu.VMEM((TP * ROWS, 128), f32),
             pltpu.VMEM((NC, SLOTS, W), bf),
             pltpu.VMEM((NC, SLOTS, W), bf),
             pltpu.VMEM((SLOTS, 2 * F), f32),
@@ -556,40 +680,30 @@
             pltpu.VMEM((2, NC, 4, ROWS, W), bf),
             pltpu.VMEM((NC, TP * ROWS, W), bf),
             pltpu.VMEM((NC, TP * ROWS, W), bf),
-            pltpu.VMEM((NC, (TP - 1) * ROWS, W), bf),
+            pltpu.VMEM((2, NC, ROWS, W), bf),
+            pltpu.VMEM((2, NC, 2, ROWS, W), bf),
             dma((NC,)),
-            dma((6,)),
-            dma((8,)),
-            dma((NC,)),
+            dma((9,)),
+            dma((11,)),
+            dma((2, NC, 2)),
             dma((NC, NZ)),
             dma,
             dma((NC,)),
             dma((NC,)),
             dma((2, NC, 4)),
+            dma((NC, TP)),
+            dma((2, NC, 2)),
             dma,
-            dma((NC,)),
+            dma,
+            dma,
         ],
         compiler_params=pltpu.CompilerParams(
-            collective_id=1, has_side_effects=True, vmem_limit_bytes=63 * 1024 * 1024
+            collective_id=1, has_side_effects=True, vmem_limit_bytes=67043328
         ),
         name="experts",
-    )(attn_rows, stream_in, norm_gain.reshape(1, D), codes, w_out, w_gate, w_up, w_down, s_gate, s_up, s_down)
-
-
-def slot_codes(routes, route_w):
-    flat = routes.reshape(-1)
-    count = flat.shape[0]
-    hits = (flat[:, None] == jnp.arange(NZ * SLAB, dtype=jnp.int32)[None, :]).astype(jnp.bfloat16)
-    at = jnp.arange(count, dtype=jnp.int32)
-    earlier = (at[None, :] < at[:, None]).astype(jnp.bfloat16)
-    before = jnp.dot(earlier, hits, preferred_element_type=jnp.float32)
-    slot = jnp.sum(before * hits.astype(jnp.float32), axis=1)
-    codes = flat.astype(jnp.float32) * CAP + slot
-    table = jnp.concatenate([codes.reshape(routes.shape).T, route_w.T], axis=0)
-    blank = jnp.zeros_like(table)
-    odd = (lax.axis_index("sp") // SLAB) % 2 == 1
-    return jnp.where(
-        odd, jnp.concatenate([blank, table], axis=1), jnp.concatenate([table, blank], axis=1)
+    )(
+        attn_rows, stream_in, norm_gain.reshape(D // 128, 128), routes.T, route_w.T,
+        w_out, w_gate, w_up, w_down, s_gate, s_up, s_down,
     )
 
 
@@ -612,10 +726,9 @@
     s_up,
     s_down,
 ):
-    codes = slot_codes(routes, route_w)
     attn_rows = attention(head_lambda, q_first, q_second, k_first, k_second, values)
     return moe(
-        attn_rows, stream_in, norm_gain, codes, w_out, w_gate, w_up, w_down, s_gate, s_up, s_down
+        attn_rows, stream_in, norm_gain, routes, route_w, w_out, w_gate, w_up, w_down, s_gate, s_up, s_down
     )
 
 

time: 224 us -> 203 us (0.906)
  Pallas kernels: 212 us -> 200 us
  local copies, waits for them, and re-layouts: 8.66 us -> 1.87 us
    pallas_call x1, Pallas kernels: 150 us -> 138 us  [moe(): pl.pallas_call(moe_kernel, out_shape=jax.ShapeDtypeStruct((ROWS, D), bf),...]
    unnamed x16 -> x1, local copies, waits for them, and re-layouts: 8.38 us -> 1.87 us
where the time goes in v3:
time: 203 us; the launch traced here: 202 us
  Pallas kernels  200 us (99%)
    pallas_call x1, Pallas kernels, moe(): pl.pallas_call(moe_kernel, out_shape=jax.ShapeDtypeStruct((ROWS, D), bf),...  138 us
    pallas_call x1, Pallas kernels, attention(): pl.pallas_call(attn_kernel, out_shape=jax.ShapeDtypeStruct((BLK, 2 * VD),...  62.3 us

profile of v3, /device:TPU:8, one launch (start us, length us, event | category | flops | bytes accessed | tf_op | source)
XLA Modules:
  0.0 201.7 jit_solution(2705015946867869529)
XLA Ops:
  0.0 62.3 %attend.1.attn_hbm = bf16[256,512]{1,0:T(8,128)(2,1)} custom-call(f32[2]{0:T(128)} %lam_ref.1, bf16[256,256]{1,0:T(8,128)(2,1)} %q1_hbm.1, bf16[256,256]{1,0:T(8,128)(2,1)} %q2_hbm.1, bf16[256,128]{1,0:T(8,128)(2,1)} %k1_hbm.1, bf16[256,128]{1,0:T(8,128)(2,1)} %k2_hbm.1, bf16[256,256]{1,0:T(8,128)(2,1)} %v_hbm.1), custom_call_target="tpu_custom_call" | custom-call | tf_op jit(solution)/shard_map/attend/pallas_call | solution.py:200
  62.3 137.5 %experts.1 = bf16[64,4096]{1,0:T(8,128)(2,1)} custom-call(bf16[256,512]{1,0:T(8,128)(2,1)} %attend.1.attn_hbm, bf16[64,4096]{1,0:T(8,128)(2,1)} %stream_hbm.1, f32[32,128]{1,0:T(8,128)} %bitcast.3, s32[4,64]{1,0:T(4,128)} %bitcast.4, f32[4,64]{1,0:T(4,128)} %bitcast.5, bf16[512,4096]{1,0:T(8,128)(2,1)} %w_out_hbm.1, bf16[1,4096,128]{2,1,0:T(8,128)(2,1)} %wg_hbm.1, ...), custom_call_target="tpu_custom_call" | custom-call | tf_op jit(solution)/shard_map/experts/pallas_call | solution.py:642
  199.9 1.9 copy.19

commit v4 on v3

--- a/solution.py
+++ b/solution.py
@@ -53,8 +53,9 @@
 
 
 def attn_kernel(
-    lam_ref, q1_hbm, q2_hbm, k1_hbm, k2_hbm, v_hbm, out_ref,
-    kv, q_s, m_s, l_s, acc_s, load_sem, send_sem, recv_sem, pair_sem,
+    lam_ref, q1_hbm, q2_hbm, k1_hbm, k2_hbm, v_hbm, routes_ref, route_w_ref,
+    out_ref, place_ref, high_ref, low_ref,
+    kv, q_s, m_s, l_s, acc_s, load_sem, send_sem, recv_sem, pair_sem, cbuf, code_sem,
 ):
     me = lax.axis_index("sp")
     c = me % 2
@@ -71,6 +72,7 @@
         "pair": at(z, y, 1 - c),
     }
     links = ("z+", "z-", "y+", "y-", "pair")
+    far = [at(z + step, y, c) for step in range(2, NZ - 1)]
 
     own = pl.multiple_of(chip * PAIR + c * BLK, BLK)
     loads = []
@@ -92,13 +94,39 @@
     barrier = pltpu.get_barrier_semaphore()
     for link in links:
         pl.semaphore_signal(barrier, inc=1, device_id=peers[link], device_id_type=pl.DeviceIdType.MESH)
+    for peer in far:
+        pl.semaphore_signal(barrier, inc=1, device_id=peer, device_id_type=pl.DeviceIdType.MESH)
 
     scale = HEAD ** (-0.5) * LOG2E
     m_s[...] = jnp.full_like(m_s, FLOOR)
     l_s[...] = jnp.zeros_like(l_s)
     acc_s[...] = jnp.zeros_like(acc_s)
 
-    pl.semaphore_wait(barrier, len(links))
+    names = lax.broadcasted_iota(jnp.int32, (NZ * SLAB, ROWS), 0)
+    hits = jnp.zeros((NZ * SLAB, ROWS), jnp.float32)
+    for j in range(TOPK):
+        hits = hits + jnp.where(routes_ref[j : j + 1, :] == names, 1.0, 0.0)
+    upper = (
+        lax.broadcasted_iota(jnp.int32, (ROWS, ROWS), 0)
+        < lax.broadcasted_iota(jnp.int32, (ROWS, ROWS), 1)
+    )
+    before = jnp.dot(
+        hits.astype(jnp.bfloat16),
+        jnp.where(upper, 1.0, 0.0).astype(jnp.bfloat16),
+        preferred_element_type=jnp.float32,
+    )
+    table = []
+    for j in range(TOPK):
+        chosen = routes_ref[j : j + 1, :]
+        taken = jnp.sum(jnp.where(chosen == names, before, 0.0), axis=0, keepdims=True)
+        table.append(chosen.astype(jnp.float32) * CAP + taken)
+    for j in range(TOPK):
+        table.append(route_w_ref[j : j + 1, :])
+    table = jnp.concatenate(table, axis=0)
+    odd = (z % 2).astype(jnp.float32)
+    cbuf[z] = jnp.concatenate([table * (1.0 - odd), table * odd], axis=1)
+
+    pl.semaphore_wait(barrier, len(links) + len(far))
     for copy in loads:
         copy.wait()
 
@@ -150,6 +178,44 @@
 
     forward(jnp.int32(0), jnp.int32(0), chip)
 
+    def tell(peer):
+        return pltpu.make_async_remote_copy(
+            src_ref=cbuf.at[z], dst_ref=cbuf.at[z], send_sem=send_sem.at[5], recv_sem=code_sem,
+            device_id=peer, device_id_type=pl.DeviceIdType.MESH,
+        )
+
+    for peer in [peers["z+"], peers["z-"]] + far:
+        tell(peer).start()
+
+    def all_told():
+        ref = cbuf.at[0 : NZ - 1]
+        return pltpu.make_async_remote_copy(
+            src_ref=ref, dst_ref=ref, send_sem=send_sem.at[5], recv_sem=code_sem,
+            device_id=peers["z+"], device_id_type=pl.DeviceIdType.MESH,
+        )
+
+    def places(q):
+        slot = lax.broadcasted_iota(jnp.int32, (SLOTS, 128), 0).astype(jnp.float32)
+        lane = lax.broadcasted_iota(jnp.int32, (SLOTS, 128), 1).astype(jnp.float32)
+        expert = jnp.floor((slot + 0.5) * (1.0 / GROUP))
+        inside = slot - expert * GROUP
+        source = jnp.floor((inside + 0.5) * (1.0 / CAP))
+        want = (z * SLAB * CAP).astype(jnp.float32) + expert * CAP + (inside - source * CAP)
+        both = cbuf[2 * q] + cbuf[2 * q + 1]
+        of_me = source == (2.0 * q.astype(jnp.float32) + jnp.floor(lane * (1.0 / ROWS)))
+        weight = jnp.zeros((SLOTS, 128), jnp.float32)
+        hit = jnp.zeros((SLOTS, 128), jnp.float32)
+        for j in range(TOPK):
+            same = of_me & (both[j : j + 1, :] == want)
+            hit = hit + jnp.where(same, 1.0, 0.0)
+            weight = weight + jnp.where(same, both[TOPK + j : TOPK + j + 1, :], 0.0)
+        span = pl.ds(pl.multiple_of(q * 128, 128), 128)
+        place_ref[:, span] = hit.astype(jnp.bfloat16)
+        turned = weight.T
+        high = turned.astype(jnp.bfloat16)
+        high_ref[span, :] = high
+        low_ref[span, :] = (turned - high.astype(jnp.float32)).astype(jnp.bfloat16)
+
     dz_table = [o[0] for o in ORDER]
     dy_table = [o[1] for o in ORDER]
 
@@ -170,6 +236,14 @@
         @pl.when(e == 1)
         def _():
             attend(chip, True)
+
+        @pl.when(e == 4)
+        def _():
+            all_told().wait_recv()
+
+        @pl.when((e >= 4) & (e < 20) & (e % 4 == 0))
+        def _():
+            places((e - 4) // 4)
 
         @pl.when((e > 1) & (last < chip))
         def _():
@@ -192,16 +266,22 @@
     for link, rows in step_counts().items():
         remote(kv.at[pl.ds(0, rows), :], link, recv_sem.at[0]).wait_send()
     remote(kv.at[pl.ds(0, NCHIP * BLK), :], "pair", recv_sem.at[0]).wait_send()
-
-
-def attention(head_lambda, q_first, q_second, k_first, k_second, values):
+    all_told().wait_send()
+
+
+def attention(head_lambda, q_first, q_second, k_first, k_second, values, routes, route_w):
     vmem = pl.BlockSpec(memory_space=pltpu.VMEM)
     hbm = pl.BlockSpec(memory_space=pl.ANY)
     return pl.pallas_call(
         attn_kernel,
-        out_shape=jax.ShapeDtypeStruct((BLK, 2 * VD), jnp.bfloat16),
-        in_specs=[pl.BlockSpec(memory_space=pltpu.SMEM)] + [hbm] * 5,
-        out_specs=vmem,
+        out_shape=[
+            jax.ShapeDtypeStruct(shape, jnp.bfloat16)
+            for shape in (
+                (BLK, 2 * VD), (SLOTS, NZ * ROWS), (NZ * ROWS, SLOTS), (NZ * ROWS, SLOTS)
+            )
+        ],
+        in_specs=[pl.BlockSpec(memory_space=pltpu.SMEM)] + [hbm] * 5 + [vmem] * 2,
+        out_specs=[vmem] * 4,
         scratch_shapes=[
             pltpu.VMEM((NCHIP * PAIR, KVW), jnp.bfloat16),
             pltpu.VMEM((2, 2 * BLK, HEAD), jnp.bfloat16),
@@ -209,15 +289,17 @@
             pltpu.VMEM((2, 2 * BLK, 128), jnp.float32),
             pltpu.VMEM((2, 2 * BLK, VD), jnp.float32),
             pltpu.SemaphoreType.DMA((7,)),
-            pltpu.SemaphoreType.DMA((5,)),
+            pltpu.SemaphoreType.DMA((6,)),
             pltpu.SemaphoreType.DMA((NCHIP,)),
             pltpu.SemaphoreType.DMA((NCHIP,)),
+            pltpu.VMEM((NZ, 8, 128), jnp.float32),
+            pltpu.SemaphoreType.DMA,
         ],
         compiler_params=pltpu.CompilerParams(
             collective_id=0, has_side_effects=True, vmem_limit_bytes=63 * 1024 * 1024
         ),
         name="attend",
-    )(head_lambda, q_first, q_second, k_first, k_second, values)
+    )(head_lambda, q_first, q_second, k_first, k_second, values, routes.T, route_w.T)
 
 
 D = 4096
@@ -232,23 +314,23 @@
 W = D // NC
 F = 128
 MESH = pl.DeviceIdType.MESH
-SUM_LAG, RESID_LAG = 3, 5
-HOP_LAGS = tuple(RESID_LAG + n for n in (3, 4, 5))
-PACK_LAG, ENTER_LAG = RESID_LAG + 6, RESID_LAG + 9
+SUM_LAG, RESID_LAG = 3, 6
+HOP_LAGS = tuple(RESID_LAG + n for n in (4, 6, 8))
+PACK_LAG, ENTER_LAG = RESID_LAG + 10, RESID_LAG + 14
 SHARE_LAG = RESID_LAG + 4
-RETURN_LAGS = (2, 4, 6, 9, 11)
+RETURN_LAGS = (3, 5, 8, 11, 14)
 
 
 def moe_kernel(
-    attn_hbm, stream_hbm, gain_hbm, routes_ref, route_w_ref,
+    attn_hbm, stream_hbm, gain_hbm, place_hbm, high_hbm, low_hbm,
     w_out_hbm, wg_hbm, wu_hbm, wd_hbm, sg_hbm, su_hbm, sd_hbm,
     out_ref,
     attn_s, stream_s, gain_s, wo, wgu, wd, sgu, sd,
-    op_all, op_out, op_in, resid_s, square_s, zbuf, cbuf, place_s, back_hi, back_lo,
+    op_all, op_out, op_in, resid_s, square_s, zbuf, place_s, back_hi, back_lo,
     turn_s, inv_own, inv_z, inv_send, inv_slot, inv_sh,
     ysend, xbuf, hid_s, hb_s, rsend, ret, part_s, rs_out, rs_in,
     sh_all, sh_out, sh_pass, sh_in,
-    wo_sem, load_sem, send_sem, op_sem, z_sem, code_sem, y_sem, r_sem, rs_sem,
+    wo_sem, load_sem, send_sem, op_sem, z_sem, y_sem, r_sem, rs_sem,
     sh_sem, shr_sem, inv_z_sem, inv_slot_sem, inv_sh_sem,
 ):
     me = lax.axis_index("sp")
@@ -303,6 +385,9 @@
         pltpu.make_async_copy(sg_hbm, sgu.at[:, 0:F], load_sem.at[3]),
         pltpu.make_async_copy(su_hbm, sgu.at[:, F : 2 * F], load_sem.at[4]),
         pltpu.make_async_copy(sd_hbm, sd, load_sem.at[5]),
+        pltpu.make_async_copy(place_hbm, place_s, load_sem.at[9]),
+        pltpu.make_async_copy(high_hbm, back_hi, load_sem.at[10]),
+        pltpu.make_async_copy(low_hbm, back_lo, load_sem.at[11]),
     ]
     for load in loads:
         load.start()
@@ -313,36 +398,11 @@
     for peer in peers:
         pl.semaphore_signal(barrier, inc=1, device_id=peer, device_id_type=MESH)
 
-    names = lax.broadcasted_iota(jnp.int32, (NZ * SLAB, ROWS), 0)
-    hits = jnp.zeros((NZ * SLAB, ROWS), jnp.float32)
-    for j in range(TOPK):
-        hits = hits + jnp.where(routes_ref[j : j + 1, :] == names, 1.0, 0.0)
-    upper = (
-        lax.broadcasted_iota(jnp.int32, (ROWS, ROWS), 0)
-        < lax.broadcasted_iota(jnp.int32, (ROWS, ROWS), 1)
-    )
-    before = jnp.dot(
-        hits.astype(jnp.bfloat16),
-        jnp.where(upper, 1.0, 0.0).astype(jnp.bfloat16),
-        preferred_element_type=jnp.float32,
-    )
-    table = []
-    for j in range(TOPK):
-        chosen = routes_ref[j : j + 1, :]
-        taken = jnp.sum(jnp.where(chosen == names, before, 0.0), axis=0, keepdims=True)
-        table.append(chosen.astype(jnp.float32) * CAP + taken)
-    for j in range(TOPK):
-        table.append(route_w_ref[j : j + 1, :])
-    table = jnp.concatenate(table, axis=0)
-    odd = (z % 2).astype(jnp.float32)
-    cbuf[z] = jnp.concatenate([table * (1.0 - odd), table * odd], axis=1)
     turn_s[...] = jnp.zeros_like(turn_s)
     square_s[...] = jnp.zeros_like(square_s)
     hid_s[...] = jnp.zeros_like(hid_s)
 
     pl.semaphore_wait(barrier, len(peers))
-    for s in range(1, NZ):
-        remote(cbuf.at[z], cbuf.at[z], 0, code_sem, to_z(s)).start()
     for load in early:
         load.wait()
 
@@ -434,31 +494,6 @@
             remote(src, land, 10, inv_slot_sem, to_slab(s)).start()
         inv_slot[rows(mine * GROUP, GROUP), :] = inv_send[rows(mine * GROUP, GROUP), :]
 
-    def places():
-        arrived(cbuf.at[0 : NZ - 1], code_sem)
-        slot = lax.broadcasted_iota(jnp.int32, (SLOTS, 128), 0).astype(jnp.float32)
-        lane = lax.broadcasted_iota(jnp.int32, (SLOTS, 128), 1).astype(jnp.float32)
-        expert = jnp.floor((slot + 0.5) * (1.0 / GROUP))
-        inside = slot - expert * GROUP
-        source = jnp.floor((inside + 0.5) * (1.0 / CAP))
-        want = (z * SLAB * CAP).astype(jnp.float32) + expert * CAP + (inside - source * CAP)
-        for q in range(NZ // 2):
-            both = cbuf[2 * q] + cbuf[2 * q + 1]
-            of_me = source == (2.0 * q + jnp.floor(lane * (1.0 / ROWS)))
-            weight = jnp.zeros((SLOTS, 128), jnp.float32)
-            hit = jnp.zeros((SLOTS, 128), jnp.float32)
-            for j in range(TOPK):
-                same = of_me & (both[j : j + 1, :] == want)
-                hit = hit + jnp.where(same, 1.0, 0.0)
-                weight = weight + jnp.where(same, both[TOPK + j : TOPK + j + 1, :], 0.0)
-            place_s[:, q * 128 : (q + 1) * 128] = hit.astype(jnp.bfloat16)
-            turned = weight.T
-            high = turned.astype(jnp.bfloat16)
-            back_hi[q * 128 : (q + 1) * 128, :] = high
-            back_lo[q * 128 : (q + 1) * 128, :] = (turned - high.astype(jnp.float32)).astype(
-                jnp.bfloat16
-            )
-
     def relay(k, step):
         below, above = (z - step + NZ) % NZ, (z + step) % NZ
         arrived(zbuf.at[k, rows(below * ROWS, ROWS), :], z_sem.at[k, below])
@@ -526,9 +561,8 @@
     def way_out(t, carry):
         guarded(t, project)
 
-        @pl.when(t == 1)
-        def _():
-            places()
+        @pl.when(t == RESID_LAG + 2)
+        def _():
             for load in loads:
                 load.wait()
 
@@ -545,7 +579,7 @@
         guarded(t - PACK_LAG, pack)
         guarded(t - ENTER_LAG, enter)
 
-        @pl.when(t == NC + 1 + RESID_LAG)
+        @pl.when(t == NC + ENTER_LAG - 4)
         def _():
             spread_inverse()
 
@@ -619,7 +653,6 @@
 
     lax.fori_loop(0, NC + b5, give_back, 0)
 
-    left(cbuf.at[0 : NZ - 1], 0)
     left(sh_all.at[:, 0 : 3 * ROWS, :], 1)
     left(sh_all.at[:, 0 : 3 * ROWS, :], 2)
     left(zbuf.at[:, 0 : 7 * ROWS, :], 3)
@@ -633,7 +666,7 @@
 
 
 def moe(
-    attn_rows, stream_in, norm_gain, routes, route_w, w_out, w_gate, w_up, w_down, s_gate, s_up, s_down
+    attn_rows, stream_in, norm_gain, places, w_out, w_gate, w_up, w_down, s_gate, s_up, s_down
 ):
     vmem = pl.BlockSpec(memory_space=pltpu.VMEM)
     hbm = pl.BlockSpec(memory_space=pl.ANY)
@@ -642,7 +675,7 @@
     return pl.pallas_call(
         moe_kernel,
         out_shape=jax.ShapeDtypeStruct((ROWS, D), bf),
-        in_specs=[hbm] * 3 + [vmem] * 2 + [hbm] * 7,
+        in_specs=[hbm] * 13,
         out_specs=vmem,
         scratch_shapes=[
             pltpu.VMEM((TP * ROWS, 2 * VD), bf),
@@ -659,7 +692,6 @@
             pltpu.VMEM((NC, ROWS, W), bf),
             pltpu.VMEM((ROWS, 128), f32),
             pltpu.VMEM((NC, NZ * ROWS, W), bf),
-            pltpu.VMEM((NZ, 8, 128), f32),
             pltpu.VMEM((SLOTS, NZ * ROWS), bf),
             pltpu.VMEM((NZ * ROWS, SLOTS), bf),
             pltpu.VMEM((NZ * ROWS, SLOTS), bf),
@@ -683,11 +715,10 @@
             pltpu.VMEM((2, NC, ROWS, W), bf),
             pltpu.VMEM((2, NC, 2, ROWS, W), bf),
             dma((NC,)),
-            dma((9,)),
+            dma((12,)),
             dma((11,)),
             dma((2, NC, 2)),
             dma((NC, NZ)),
-            dma,
             dma((NC,)),
             dma((NC,)),
             dma((2, NC, 4)),
@@ -702,7 +733,7 @@
         ),
         name="experts",
     )(
-        attn_rows, stream_in, norm_gain.reshape(D // 128, 128), routes.T, route_w.T,
+        attn_rows, stream_in, norm_gain.reshape(D // 128, 128), *places,
         w_out, w_gate, w_up, w_down, s_gate, s_up, s_down,
     )
 
@@ -726,9 +757,11 @@
     s_up,
     s_down,
 ):
-    attn_rows = attention(head_lambda, q_first, q_second, k_first, k_second, values)
+    attn_rows, *places = attention(
+        head_lambda, q_first, q_second, k_first, k_second, values, routes, route_w
+    )
     return moe(
-        attn_rows, stream_in, norm_gain, routes, route_w, w_out, w_gate, w_up, w_down, s_gate, s_up, s_down
+        attn_rows, stream_in, norm_gain, places, w_out, w_gate, w_up, w_down, s_gate, s_up, s_down
     )
 
 

time: 203 us -> 200 us (0.985)
    pallas_call x1, Pallas kernels: 138 us -> 132 us  [moe(): pl.pallas_call(moe_kernel, out_shape=jax.ShapeDtypeStruct((ROWS, D), bf),...]
    pallas_call x1, Pallas kernels: 62.3 us -> 65.7 us  [attention(): pl.pallas_call(attn_kernel, out_shape=[jax.ShapeDtypeStruct(shape, jnp.bf...]
where the time goes in v4:
time: 200 us
  Pallas kernels  198 us (99%)
    pallas_call x1, Pallas kernels, moe(): pl.pallas_call(moe_kernel, out_shape=jax.ShapeDtypeStruct((ROWS, D), bf),...  132 us
    pallas_call x1, Pallas kernels, attention(): pl.pallas_call(attn_kernel, out_shape=[jax.ShapeDtypeStruct(shape, jnp.bf...  65.7 us

profile of v4, /device:TPU:8, one launch (start us, length us, event | category | flops | bytes accessed | tf_op | source)
XLA Modules:
  0.0 199.5 jit_solution(15389439316998343910)
XLA Ops:
  0.0 65.7 %attend.1 = (bf16[256,512]{1,0:T(8,128)(2,1)}, bf16[384,512]{1,0:T(8,128)(2,1)}, bf16[512,384]{1,0:T(8,128)(2,1)}, bf16[512,384]{1,0:T(8,128)(2,1)}) custom-call(f32[2]{0:T(128)} %lam_ref.1, bf16[256,256]{1,0:T(8,128)(2,1)} %q1_hbm.1, bf16[256,256]{1,0:T(8,128)(2,1)} %q2_hbm.1, bf16[256,128]{1,0:T(8,128)(2,1)} %k1_hbm.1, bf16[256,128]{1,0:T(8,128)(2,1)} %k2_hbm.1, ...), custom_call_target="tpu_custom_call" | custom-call | tf_op jit(solution)/shard_map/attend/pallas_call | solution.py:275
  65.7 131.9 %experts.1 = bf16[64,4096]{1,0:T(8,128)(2,1)} custom-call(bf16[256,512]{1,0:T(8,128)(2,1)} %get-tuple-element.9.attn_hbm, bf16[64,4096]{1,0:T(8,128)(2,1)} %stream_hbm.1, f32[32,128]{1,0:T(8,128)} %bitcast.3, bf16[384,512]{1,0:T(8,128)(2,1)} %get-tuple-element.10.place_hbm, bf16[512,384]{1,0:T(8,128)(2,1)} %get-tuple-element.11.high_hbm, ...), custom_call_target="tpu_custom_call" | custom-call | tf_op jit(solution)/shard_map/experts/pallas_call | solution.py:675
  197.6 1.9 copy.19

commit v5 on v4

--- a/solution.py
+++ b/solution.py
@@ -152,19 +152,23 @@
     def attend(src_chip, masked):
         base = pl.multiple_of(src_chip * PAIR, PAIR)
         value = kv[pl.ds(base, PAIR), 256:512]
+        scores, olds = [], []
         for k in range(2):
             key = kv[pl.ds(base, PAIR), k * HEAD : (k + 1) * HEAD]
-            scores = lax.dot_general(
+            scores.append(lax.dot_general(
                 q_s[k], key, (((1,), (1,)), ((), ())), preferred_element_type=jnp.float32
-            ) * scale
+            ) * scale)
+            olds.append(m_s[k])
+        fades, packs = [], []
+        for k in range(2):
+            score = scores[k]
             if masked:
-                q_pos = lax.broadcasted_iota(jnp.int32, scores.shape, 0) % BLK + c * BLK
-                k_pos = lax.broadcasted_iota(jnp.int32, scores.shape, 1)
-                scores = jnp.where(k_pos <= q_pos, scores, FLOOR)
-            old = m_s[k]
-            new = jnp.maximum(old, jnp.max(scores, axis=1, keepdims=True))
-            fade = jnp.exp2(old - new)
-            weights = jnp.exp2(scores - jnp.tile(new, (1, PAIR // 128)))
+                q_pos = lax.broadcasted_iota(jnp.int32, score.shape, 0) % BLK + c * BLK
+                k_pos = lax.broadcasted_iota(jnp.int32, score.shape, 1)
+                score = jnp.where(k_pos <= q_pos, score, FLOOR)
+            new = jnp.maximum(olds[k], jnp.max(score, axis=1, keepdims=True))
+            fade = jnp.exp2(olds[k] - new)
+            weights = jnp.exp2(score - jnp.tile(new, (1, PAIR // 128)))
             if masked:
                 weights = jnp.where(k_pos <= q_pos, weights, 0.0)
             part = weights[:, 0:128]
@@ -172,8 +176,11 @@
                 part = part + weights[:, t * 128 : (t + 1) * 128]
             m_s[k] = new
             l_s[k] = l_s[k] * fade + part
-            acc_s[k] = acc_s[k] * jnp.tile(fade, (1, VD // 128)) + jnp.dot(
-                weights.astype(jnp.bfloat16), value, preferred_element_type=jnp.float32
+            fades.append(fade)
+            packs.append(weights.astype(jnp.bfloat16))
+        for k in range(2):
+            acc_s[k] = acc_s[k] * jnp.tile(fades[k], (1, VD // 128)) + jnp.dot(
+                packs[k], value, preferred_element_type=jnp.float32
             )
 
     forward(jnp.int32(0), jnp.int32(0), chip)

time: 200 us -> 199 us (level)
  no operation moved by 1% of the time
where the time goes in v5:
time: 199 us; the launch traced here: 198 us
  Pallas kernels  197 us (99%)
    pallas_call x1, Pallas kernels, moe(): pl.pallas_call(moe_kernel, out_shape=jax.ShapeDtypeStruct((ROWS, D), bf),...  132 us
    pallas_call x1, Pallas kernels, attention(): pl.pallas_call(attn_kernel, out_shape=[jax.ShapeDtypeStruct(shape, jnp.bf...  64.9 us

profile of v5, /device:TPU:8, one launch (start us, length us, event | category | flops | bytes accessed | tf_op | source)
XLA Modules:
  0.0 198.5 jit_solution(8716103728594979857)
XLA Ops:
  0.0 64.9 %attend.1 = (bf16[256,512]{1,0:T(8,128)(2,1)}, bf16[384,512]{1,0:T(8,128)(2,1)}, bf16[512,384]{1,0:T(8,128)(2,1)}, bf16[512,384]{1,0:T(8,128)(2,1)}) custom-call(f32[2]{0:T(128)} %lam_ref.1, bf16[256,256]{1,0:T(8,128)(2,1)} %q1_hbm.1, bf16[256,256]{1,0:T(8,128)(2,1)} %q2_hbm.1, bf16[256,128]{1,0:T(8,128)(2,1)} %k1_hbm.1, bf16[256,128]{1,0:T(8,128)(2,1)} %k2_hbm.1, ...), custom_call_target="tpu_custom_call" | custom-call | tf_op jit(solution)/shard_map/attend/pallas_call | solution.py:282
  64.9 131.7 %experts.1 = bf16[64,4096]{1,0:T(8,128)(2,1)} custom-call(bf16[256,512]{1,0:T(8,128)(2,1)} %get-tuple-element.9.attn_hbm, bf16[64,4096]{1,0:T(8,128)(2,1)} %stream_hbm.1, f32[32,128]{1,0:T(8,128)} %bitcast.3, bf16[384,512]{1,0:T(8,128)(2,1)} %get-tuple-element.10.place_hbm, bf16[512,384]{1,0:T(8,128)(2,1)} %get-tuple-element.11.high_hbm, ...), custom_call_target="tpu_custom_call" | custom-call | tf_op jit(solution)/shard_map/experts/pallas_call | solution.py:682
  196.6 1.9 copy.19
